TPU v7x, 32 devices: a whole 2x2x4 slice. The times are simulated.
32 devices in a mesh: sp: 8 (over z, x), tp: 4 (over y, core).
Axes of the slice: x: 2, y: 2, z: 4, core: 2. Of those that a mesh axis runs over, the one named last changes fastest.
Arguments:
- moe_input: bfloat16 [1536, 2048], P('sp'), may hold values from -6 to 6
- out_grad: bfloat16 [1536, 2048], P('sp', 'tp'), may hold values from -6 to 6
- expert_ids: int32 [1536, 2], P('sp'), may hold values from 0 to 7, all different within a row; in each aligned block of 192 rows (0 to 191, 192 to 383, ...) at most 60 rows name the same one
- expert_weights: float32 [1536, 2], P('sp'), may hold values from 0.1 to 0.9
- w_gate: bfloat16 [8, 2048, 2048], P('sp', None, 'tp'), may hold values from -0.125 to 0.125
- w_up: bfloat16 [8, 2048, 2048], P('sp', None, 'tp'), may hold values from -0.125 to 0.125
- w_down: bfloat16 [8, 2048, 2048], P('sp', 'tp'), may hold values from -0.125 to 0.125
- out_proj: bfloat16 [1536, 2048], P('tp'), may hold values from -0.15625 to 0.15625
- retained: bfloat16 [1536, 1536], P('sp', 'tp'), may hold values from -6 to 6
- queries: bfloat16 [1536, 768], P('sp', 'tp'), may hold values from -6 to 6
- keys: bfloat16 [1536, 768], P('sp', 'tp'), may hold values from -0.86328125 to 0.86328125
- values: bfloat16 [1536, 1536], P('sp', 'tp'), may hold values from -6 to 6
- log_decay: float32 [1536, 16], P('sp', 'tp'), may hold values from -1 to 0
- incoming_state: float32 [8, 16, 48, 96], P('sp', 'tp'), may hold values from -6 to 6
Outputs:
- w_gate_grad: bfloat16 [8, 2048, 2048], P('sp', None, 'tp')
- w_up_grad: bfloat16 [8, 2048, 2048], P('sp', None, 'tp')
- w_down_grad: bfloat16 [8, 2048, 2048], P('sp', 'tp')
- out_proj_grad: float32 [2048, 1536], P('sp', 'tp')
- query_grad: bfloat16 [1536, 768], P('sp', 'tp')
- key_grad: bfloat16 [1536, 768], P('sp', 'tp')
- value_grad: bfloat16 [1536, 1536], P('sp', 'tp')
Inputs may be any that keep to these rules, and one draw needn't show every extreme that they name: `expert_ids`: in each aligned block of 192 positions no expert is named by more than 60 of the block's assignments, a bound that some block reaches.
All inputs are finite; a program needn't handle non-finite values.
Results may differ from a plain program's by a relative error of at most 0.02.
Values may be sent and summed in bfloat16 or wider, within the bound.
No kernel may reach another device: no remote copies, remote signals or barrier semaphores. Data moves between devices by JAX's collectives and lax.ppermute only.
A program may use at most 64 MiB of HBM per device.

v0:
```python
import jax
import jax.numpy as jnp
from jax import lax
from jax.sharding import PartitionSpec as P


def carried_in(x, axis, combine, identity):
    devices, place = (lax.axis_size(axis), lax.axis_index(axis))
    everything = jax.tree.map(lambda part: lax.all_gather(part, axis), x)
    start = jax.tree.map(
        lambda part, zero: jnp.broadcast_to(jnp.asarray(zero, part.dtype), part.shape), x, identity
    )

    def lap(k, before):
        at = devices - 1 - k
        reached = at > place
        new = combine(before, jax.tree.map(lambda part: part[at], everything))
        return jax.tree.map(lambda a, b: jnp.where(reached, a, b), new, before)

    return lax.fori_loop(0, devices, lap, start)


def expert_back(rows, grad, gate_w, up_w, down_w):
    f32 = jnp.float32
    bf16 = jnp.bfloat16
    gate = jnp.dot(rows, gate_w, preferred_element_type=f32)
    up = jnp.dot(rows, up_w, preferred_element_type=f32)
    sig = jax.nn.sigmoid(gate)
    swish = gate * sig
    act = (swish * up).astype(bf16)
    across = (((1,), (1,)), ((), ()))
    along = (((0,), (0,)), ((), ()))
    act_grad = lax.dot_general(grad, down_w, across, preferred_element_type=f32)
    gate_grad = (act_grad * up * sig * (1.0 + gate * (1.0 - sig))).astype(bf16)
    up_grad = (act_grad * swish).astype(bf16)
    down_grad = lax.dot_general(act, grad, along, preferred_element_type=f32).astype(bf16)
    gate_w_grad = lax.dot_general(rows, gate_grad, along, preferred_element_type=f32).astype(bf16)
    up_w_grad = lax.dot_general(rows, up_grad, along, preferred_element_type=f32).astype(bf16)
    partial_value = lax.dot_general(
        gate_grad, gate_w, across, preferred_element_type=f32
    ) + lax.dot_general(up_grad, up_w, across, preferred_element_type=f32)
    return (gate_w_grad, up_w_grad, down_grad, partial_value)


def combine_states(earlier, later):
    return (later[0] * earlier[0], later[1] + later[0][:, None, None] * earlier[1])


def on_device(
    moe_input,
    out_grad,
    expert_ids,
    expert_weights,
    w_gate,
    w_up,
    w_down,
    out_proj,
    retained,
    queries,
    keys,
    values,
    log_decay,
    incoming_state,
):
    f32 = jnp.float32
    bf16 = jnp.bfloat16
    upper_limit = lax.Precision.HIGHEST
    tokens_here = moe_input.shape[0]
    width = moe_input.shape[1]
    sp_count = lax.axis_size("sp")
    tp_count = lax.axis_size("tp")
    capacity = 5 * tokens_here // (2 * sp_count)
    slot_count = sp_count * capacity
    flat_ids = expert_ids.reshape(-1)
    flat_weights = expert_weights.reshape(-1)
    onehot = (flat_ids[:, None] == jnp.arange(sp_count, dtype=jnp.int32)[None, :]).astype(jnp.int32)
    ranks = jnp.sum((jnp.cumsum(onehot, axis=0) - onehot) * onehot, axis=1)
    slot_of = flat_ids * capacity + ranks
    hits = jnp.arange(slot_count, dtype=jnp.int32)[:, None] == slot_of[None, :]
    picker = jnp.any(hits.reshape(slot_count, tokens_here, 2), axis=2).astype(bf16)
    slot_weight = jnp.sum(jnp.where(hits, flat_weights[None, :], 0.0), axis=1)
    along = (((0,), (0,)), ((), ()))
    column_count = width // tp_count
    own_rows = lax.dynamic_slice_in_dim(
        moe_input, lax.axis_index("tp") * column_count, column_count, 1
    )
    send_rows = jnp.dot(picker, own_rows, preferred_element_type=f32).astype(bf16)
    send_grad = (
        jnp.dot(picker, out_grad, preferred_element_type=f32) * slot_weight[:, None]
    ).astype(bf16)
    part_rows, part_grad = (
        lax.all_to_all(send_rows, "sp", split_axis=0, concat_axis=0, tiled=True),
        lax.all_to_all(send_grad, "sp", split_axis=0, concat_axis=0, tiled=True),
    )
    recv_rows, recv_grad = (
        lax.all_gather(part_rows, "tp", axis=1, tiled=True),
        lax.all_gather(part_grad, "tp", axis=1, tiled=True),
    )
    gate_w_grad, up_w_grad, down_grad, partial_value = expert_back(
        recv_rows, recv_grad, w_gate[0], w_up[0], w_down[0]
    )
    share = (
        lax.psum_scatter(partial_value.astype(jnp.bfloat16), "tp", scatter_dimension=1, tiled=True)
        .astype(jnp.float32)
        .astype(bf16)
    )
    returned = lax.all_to_all(share, "sp", split_axis=0, concat_axis=0, tiled=True)
    token_grad = lax.dot_general(picker, returned, along, preferred_element_type=f32)
    stream_part = (out_grad.astype(f32) + token_grad).astype(bf16)
    stream = lax.all_gather(stream_part, "tp", axis=1, tiled=True)
    ret_grad = lax.dot_general(
        stream, out_proj, (((1,), (1,)), ((), ())), preferred_element_type=f32
    ).astype(bf16)
    out_proj_grad = lax.psum_scatter(
        lax.dot_general(stream, retained, along, preferred_element_type=f32).astype(jnp.bfloat16),
        "sp",
        scatter_dimension=0,
        tiled=True,
    ).astype(jnp.float32)
    heads_here = log_decay.shape[1]
    key_dim = queries.shape[1] // heads_here
    value_dim = values.shape[1] // heads_here
    query_rows = queries.astype(f32).reshape(tokens_here, heads_here, key_dim)
    key_matrix = keys.astype(f32).reshape(tokens_here, heads_here, key_dim)
    value_matrix = values.astype(f32).reshape(tokens_here, heads_here, value_dim)
    incoming_gradient = ret_grad.astype(f32).reshape(tokens_here, heads_here, value_dim)
    running_total = jnp.cumsum(log_decay, axis=0)
    last_sum = running_total[-1]
    place = jnp.arange(tokens_here)
    causal = (place[:, None] >= place[None, :])[:, :, None]
    diff = running_total[:, None, :] - running_total[None, :, :]
    decay = jnp.where(causal, jnp.exp(jnp.minimum(diff, 0.0)), 0.0)
    scores = jnp.einsum("thk,shk->tsh", query_rows, key_matrix, precision=upper_limit) * decay
    prob_grad = (
        jnp.einsum("thv,shv->tsh", incoming_gradient, value_matrix, precision=upper_limit) * decay
    )
    added_input = jnp.einsum(
        "yb,ybm,ybx->bmx",
        jnp.exp(running_total),
        query_rows,
        incoming_gradient,
        precision=upper_limit,
    )
    block_multiplier = jnp.exp(last_sum)
    _, state_gradient = carried_in(
        (block_multiplier, added_input),
        "sp",
        combine_states,
        (jnp.ones_like(block_multiplier), jnp.zeros_like(added_input)),
    )
    tail = jnp.exp(last_sum[None, :] - running_total)[..., None]
    query_grad = jnp.einsum("tsh,shk->thk", prob_grad, key_matrix, precision=upper_limit) + jnp.exp(
        running_total
    )[..., None] * jnp.einsum(
        "ybc,bfc->ybf", incoming_gradient, incoming_state[0], precision=upper_limit
    )
    key_grad = jnp.einsum(
        "tsh,thk->shk", prob_grad, query_rows, precision=upper_limit
    ) + tail * jnp.einsum("rgd,gnd->rgn", value_matrix, state_gradient, precision=upper_limit)
    value_grad = jnp.einsum(
        "tsh,thv->shv", scores, incoming_gradient, precision=upper_limit
    ) + tail * jnp.einsum("bgi,gie->bge", key_matrix, state_gradient, precision=upper_limit)
    return (
        gate_w_grad[None],
        up_w_grad[None],
        down_grad[None],
        out_proj_grad,
        query_grad.reshape(tokens_here, -1).astype(bf16),
        key_grad.reshape(tokens_here, -1).astype(bf16),
        value_grad.reshape(tokens_here, -1).astype(bf16),
    )


def solution(mesh):
    placed = (
        P("sp", None),
        P("sp", "tp"),
        P("sp", None),
        P("sp", None),
        P("sp", None, "tp"),
        P("sp", None, "tp"),
        P("sp", "tp", None),
        P("tp", None),
        P("sp", "tp"),
        P("sp", "tp"),
        P("sp", "tp"),
        P("sp", "tp"),
        P("sp", "tp"),
        P("sp", "tp", None, None),
    )
    return jax.shard_map(
        on_device,
        mesh=mesh,
        in_specs=placed,
        out_specs=(
            P("sp", None, "tp"),
            P("sp", None, "tp"),
            P("sp", "tp", None),
            P("sp", "tp"),
            P("sp", "tp"),
            P("sp", "tp"),
            P("sp", "tp"),
        ),
        check_vma=False,
    )
```

profile of v0, /device:TPU:0, one launch (start us, length us, event | category | flops | bytes accessed | tf_op | source)
XLA Modules:
  0.0 227.4 jit_solution(18031763401095627964)
XLA Ops:
  10.8 1.3 convolution_convert_fusion.4
  12.2 21.6 %all_to_all.36 = bf16[8,60,512]{2,1,0:T(8,128)(2,1)S(1)} all-to-all(bf16[8,60,512]{2,1,0:T(8,128)(2,1)S(1)} %all_to_all.24), channel_id=1, replica_groups=mesh['sp'=8,'tp'=4] {'sp'}, dimensions={0} | all-to-all | bytes 983040 | tf_op jit(solution)/shard_map/all_to_all | solution.py:92
  35.7 17.5 %all_to_all.37 = bf16[8,60,512]{2,1,0:T(8,128)(2,1)S(1)} all-to-all(bf16[8,60,512]{2,1,0:T(8,128)(2,1)S(1)} %all_to_all.27), channel_id=1, replica_groups=mesh['sp'=8,'tp'=4] {'sp'}, dimensions={0} | all-to-all | bytes 983040 | tf_op jit(solution)/shard_map/all_to_all | solution.py:93
  54.2 1.6 all-gather.5.cloned.1.call-done
  55.8 3.8 %fusion.6 = f32[480,512]{1,0:T(8,128)} fusion(bf16[480,2048]{1,0:T(8,128)(2,1)} %all-gather.5.cloned.1.call-done, bf16[1,2048,512]{2,1,0:T(8,128)(2,1)S(1)} %copy-done), kind=kOutput, calls=%fused_computation.13 | convolution fusion | flops 1006632960 | bytes 5046272 | tf_op jit(solution)/shard_map/dot_general | solution.py:26
  59.6 2.2 fusion.9
  61.7 18.0 %all-gather.7.cloned.1.call-done = bf16[480,2048]{1,0:T(8,128)(2,1)} async-done(((bf16[480,512]{1,0:T(8,128)(2,1)}), bf16[480,2048]{1,0:T(8,128)(2,1)}) %all-gather.7.cloned.1.call-update) | async-done | bytes 1966096 | tf_op jit(solution)/shard_map/all_gather | solution.py:97
  79.7 4.2 %multiply_convert_fusion.1 = (bf16[480,512]{1,0:T(8,128)(2,1)S(1)}, bf16[480,512]{1,0:T(8,128)(2,1)S(1)}) fusion(f32[480,512]{1,0:T(8,128)} %fusion.6, f32[480,512]{1,0:T(8,128)} %fusion.9, bf16[480,2048]{1,0:T(8,128)(2,1)} %all-gather.7.cloned.1.call-done, bf16[1,512,2048]{2,1,0:T(8,128)(2,1)} %param.22), kind=kOutput, calls=%fused_computation.46 | convolution fusion | flops 1009827840 | bytes 7012352 | tf_op jit(solution)/shard_map/dot_general | solution.py:33
  84.0 1.2 fusion.4
  85.7 2.5 %add_convert_fusion = bf16[480,2048]{1,0:T(8,128)(2,1)} fusion(f32[480,2048]{1,0:T(8,128)S(1)} %fusion.4, bf16[480,512]{1,0:T(8,128)(2,1)S(1)} %get-tuple-element.242, bf16[1,2048,512]{2,1,0:T(8,128)(2,1)S(1)} %copy-done.2), kind=kOutput, calls=%fused_computation.3 | convolution fusion | flops 1008599040 | bytes 8486912 | tf_op jit(solution)/shard_map/dot_general | solution.py:41
  88.3 1.2 reduce-window.16
  91.2 20.5 %all-gather.1 = f32[8,1,4]{2,1,0:T(1,128)S(1)} all-gather(f32[1,1,4]{2,1,0:T(1,128)S(1)} %bitcast.153), channel_id=1, replica_groups=mesh['sp'=8,'tp'=4] {'sp'}, dimensions={0}, use_global_device_ids=true | all-gather | bytes 144 | tf_op jit(solution)/shard_map/all_gather | solution.py:9
  112.3 1.3 fusion.13
  113.6 5.2 %reduce-scatter.3.cloned.1.call-done = bf16[480,512]{1,0:T(8,128)(2,1)} async-done(((bf16[480,2048]{1,0:T(8,128)(2,1)}), bf16[480,512]{1,0:T(8,128)(2,1)}) %reduce-scatter.3.cloned.1.call-update) | async-done | bytes 491536 | tf_op jit(solution)/shard_map/reduce_scatter | solution.py:103
  118.8 1.9 all_to_all.30
  120.7 5.5 %all-to-all-start.2 = ((bf16[8,60,512]{2,1,0:T(8,128)(2,1)}), bf16[8,60,512]{2,1,0:T(8,128)(2,1)S(1)}, u32[]{:S(2)}, u32[]{:S(2)}) async-start(bf16[8,60,512]{2,1,0:T(8,128)(2,1)} %all_to_all.30), calls=%async_computation.3 | async-start | bytes 1048576 | tf_op jit(solution)/shard_map/all_to_all | solution.py:107
  126.5 4.3 %fusion.1 = bf16[1,2048,512]{2,1,0:T(8,128)(2,1)} fusion(bf16[480,2048]{1,0:T(8,128)(2,1)} %all-gather.5.cloned.1.call-done, bf16[480,512]{1,0:T(8,128)(2,1)S(1)} %get-tuple-element.243), kind=kOutput, calls=%fused_computation.8 | convolution fusion | flops 1007681536 | bytes 4554752 | tf_op jit(solution)/shard_map/dot_general | solution.py:37
  130.8 2.6 %fusion.2 = bf16[1,2048,512]{2,1,0:T(8,128)(2,1)} fusion(bf16[480,2048]{1,0:T(8,128)(2,1)S(1)} %copy-done.14, bf16[480,512]{1,0:T(8,128)(2,1)S(1)} %copy-done.4), kind=kOutput, calls=%fused_computation.9 | convolution fusion | flops 1007681536 | bytes 4554752 | tf_op jit(solution)/shard_map/dot_general | solution.py:38
  133.4 2.7 %fusion.3 = bf16[1,512,2048]{2,1,0:T(8,128)(2,1)} fusion(bf16[480,2048]{1,0:T(8,128)(2,1)S(1)} %copy-done.15, f32[480,512]{1,0:T(8,128)S(1)} %copy-done.17, f32[480,512]{1,0:T(8,128)S(1)} %copy-done.16), kind=kOutput, calls=%fused_computation.10 | convolution fusion | flops 1009156096 | bytes 6029312 | tf_op jit(solution)/shard_map/dot_general | solution.py:36
  136.1 4.4 %all-to-all-done.2 = bf16[8,60,512]{2,1,0:T(8,128)(2,1)S(1)} async-done(((bf16[8,60,512]{2,1,0:T(8,128)(2,1)}), bf16[8,60,512]{2,1,0:T(8,128)(2,1)S(1)}, u32[]{:S(2)}, u32[]{:S(2)}) %all-to-all-start.2) | async-done | bytes 491552 | tf_op jit(solution)/shard_map/all_to_all | solution.py:107
  140.6 1.2 fusion.18
  141.8 7.7 %all_gather.21 = bf16[192,2048]{1,0:T(8,128)(2,1)S(1)} all-gather(bf16[192,512]{1,0:T(8,128)(2,1)S(1)} %fusion.18), channel_id=1, replica_groups=mesh['sp'=8,'tp'=4] {'tp'}, dimensions={1}, use_global_device_ids=true | all-gather | bytes 983040 | tf_op jit(solution)/shard_map/all_gather | solution.py:110
  149.5 2.8 %convolution_convert_fusion.3 = bf16[2048,384]{1,0:T(8,128)(2,1)} fusion(bf16[192,2048]{1,0:T(8,128)(2,1)S(1)} %all_gather.21, bf16[192,384]{1,0:T(8,128)(2,1)} %param.24), kind=kOutput, calls=%fused_computation.7 | convolution fusion | flops 302776320 | bytes 2506752 | tf_op jit(solution)/shard_map/dot_general | solution.py:115
  152.3 2.1 convolution_convert_fusion.5
  155.1 1.3 fusion.14
  157.6 1.6 copy.162
  159.3 35.0 %all-gather = f32[32,48,96]{2,1,0:T(8,128)} all-gather(f32[4,48,96]{2,1,0:T(8,128)S(1)} %fusion.28), channel_id=2, replica_groups=mesh['sp'=8,'tp'=4] {'sp'}, dimensions={0}, use_global_device_ids=true | all-gather | bytes 663552 | tf_op jit(solution)/shard_map/all_gather | solution.py:9
  194.3 8.2 %while.16 = (s32[]{:T(128)}, f32[4,48,96]{2,1,0:T(8,128)S(1)}, s32[]{:T(128)}, f32[8,4,48,96]{3,2,1,0:T(8,128)}, f32[8,4]{1,0:T(8,128)S(1)}, /*index=5*/s32[]{:T(128)}, s32[]{:T(128)}, s32[]{:T(128)}, s32[]{:T(128)}) while((s32[]{:T(128)}, f32[4,48,96]{2,1,0:T(8,128)S(1)}, s32[]{:T(128)}, f32[8,4,48,96]{3,2,1,0:T(8,128)}, ...), condition=%wide.region_10.11_spmd.clone, body=%wide.region_9.10_spmd.clone.sunk | while | flops 73736 | bytes 221407 | solution.py:20
  202.5 1.4 fusion.22
  205.1 1.6 convolution_bitcast_fusion.3
  207.8 11.4 %reduce-scatter.5.cloned.1.call-done = bf16[256,384]{1,0:T(8,128)(2,1)} async-done(((bf16[2048,384]{1,0:T(8,128)(2,1)}), bf16[256,384]{1,0:T(8,128)(2,1)}) %reduce-scatter.5.cloned.1.call-update) | async-done | bytes 196624 | tf_op jit(solution)/shard_map/reduce_scatter | solution.py:114
  219.2 1.7 convert_element_type.88
  (106 shorter events, 21.7 us)
Async XLA Ops:
  7.2 48.6 %copy-start = (bf16[1,2048,512]{2,1,0:T(8,128)(2,1)S(1)}, bf16[1,2048,512]{2,1,0:T(8,128)(2,1)}, u32[]{:S(2)}) copy-start(bf16[1,2048,512]{2,1,0:T(8,128)(2,1)} %param.20) | copy-start | bytes 6291460
  7.2 48.6 %all-gather.5.cloned.1.call-start = ((), (), s32[]{:S(2)}) async-start(), calls=%async_computation.5 | async-start | bytes 2457600 | tf_op jit(solution)/shard_map/all_gather | solution.py:96
  10.8 24.0 %copy-start.12 = (f32[192,2]{0,1:T(2,128)S(1)}, f32[192,2]{0,1:T(2,128)}, u32[]{:S(2)}) copy-start(f32[192,2]{0,1:T(2,128)} %param.19) | copy-start | bytes 4612
  10.8 24.4 %copy-start.5 = (bf16[192,512]{1,0:T(8,128)(2,1)S(1)}, bf16[192,512]{1,0:T(8,128)(2,1)}, u32[]{:S(2)}) copy-start(bf16[192,512]{1,0:T(8,128)(2,1)} %param.17) | copy-start | bytes 589828
  34.7 45.0 %all-gather.7.cloned.1.call-start = ((), (), s32[]{:S(2)}) async-start(), calls=%async_computation.6 | async-start | bytes 2457600 | tf_op jit(solution)/shard_map/all_gather | solution.py:97
  54.1 64.7 %reduce-scatter.3.cloned.1.call-start = ((), (), s32[]{:S(2)}) async-start(), calls=%async_computation.7 | async-start | bytes 2457600 | tf_op jit(solution)/shard_map/reduce_scatter | solution.py:103
  55.7 3.8 %copy-start.1 = (bf16[1,2048,512]{2,1,0:T(8,128)(2,1)S(1)}, bf16[1,2048,512]{2,1,0:T(8,128)(2,1)}, u32[]{:S(2)}) copy-start(bf16[1,2048,512]{2,1,0:T(8,128)(2,1)} %param.21) | copy-start | bytes 6291460
  55.7 3.8 %copy-start.13 = (bf16[480,2048]{1,0:T(8,128)(2,1)S(1)}, bf16[480,2048]{1,0:T(8,128)(2,1)}, u32[]{:S(2)}) copy-start(bf16[480,2048]{1,0:T(8,128)(2,1)} %all-gather.5.cloned.1.call-done) | copy-start | bytes 5898244
  83.9 1.2 copy-start.3
  83.9 1.8 copy-start.2
  85.7 2.5 %copy-start.11 = (f32[192,4]{0,1:T(4,128)S(1)}, f32[192,4]{0,1:T(4,128)}, u32[]{:S(2)}) copy-start(f32[192,4]{0,1:T(4,128)} %param.28) | copy-start | bytes 9220
  88.2 1.7 copy-start.6
  88.2 2.5 %copy-start.7 = (bf16[192,192]{1,0:T(8,128)(2,1)S(1)}, bf16[192,192]{1,0:T(8,128)(2,1)}, u32[]{:S(2)}) copy-start(bf16[192,192]{1,0:T(8,128)(2,1)} %param.26) | copy-start | bytes 221188
  88.2 2.6 %copy-start.8 = (bf16[192,192]{1,0:T(8,128)(2,1)S(1)}, bf16[192,192]{1,0:T(8,128)(2,1)}, u32[]{:S(2)}) copy-start(bf16[192,192]{1,0:T(8,128)(2,1)} %param.25) | copy-start | bytes 221188
  111.7 0.6 copy-start.10
  120.7 19.8 %all-to-all-start.2 = ((bf16[8,60,512]{2,1,0:T(8,128)(2,1)}), bf16[8,60,512]{2,1,0:T(8,128)(2,1)S(1)}, u32[]{:S(2)}, u32[]{:S(2)}) async-start(bf16[8,60,512]{2,1,0:T(8,128)(2,1)} %all_to_all.30), calls=%async_computation.3 | async-start | bytes 1048576 | tf_op jit(solution)/shard_map/all_to_all | solution.py:107
  126.2 93.0 %reduce-scatter.5.cloned.1.call-start = ((), (), s32[]{:S(2)}) async-start(), calls=%async_computation.8 | async-start | bytes 1769472 | tf_op jit(solution)/shard_map/reduce_scatter | solution.py:114
  126.4 4.3 %copy-start.4 = (bf16[480,512]{1,0:T(8,128)(2,1)S(1)}, bf16[480,512]{1,0:T(8,128)(2,1)}, u32[]{:S(2)}) copy-start(bf16[480,512]{1,0:T(8,128)(2,1)} %copy-done.3) | copy-start | bytes 1474564
  126.5 4.3 %copy-start.14 = (bf16[480,2048]{1,0:T(8,128)(2,1)S(1)}, bf16[480,2048]{1,0:T(8,128)(2,1)}, u32[]{:S(2)}) copy-start(bf16[480,2048]{1,0:T(8,128)(2,1)} %all-gather.5.cloned.1.call-done) | copy-start | bytes 5898244
  130.8 2.7 %copy-start.15 = (bf16[480,2048]{1,0:T(8,128)(2,1)S(1)}, bf16[480,2048]{1,0:T(8,128)(2,1)}, u32[]{:S(2)}) copy-start(bf16[480,2048]{1,0:T(8,128)(2,1)} %all-gather.7.cloned.1.call-done) | copy-start | bytes 5898244
  130.8 2.7 %copy-start.16 = (f32[480,512]{1,0:T(8,128)S(1)}, f32[480,512]{1,0:T(8,128)}, u32[]{:S(2)}) copy-start(f32[480,512]{1,0:T(8,128)} %fusion.6) | copy-start | bytes 2949124
  130.8 2.7 %copy-start.17 = (f32[480,512]{1,0:T(8,128)S(1)}, f32[480,512]{1,0:T(8,128)}, u32[]{:S(2)}) copy-start(f32[480,512]{1,0:T(8,128)} %fusion.9) | copy-start | bytes 2949124
  152.3 2.6 %copy-start.9 = (f32[1,4,48,96]{3,2,1,0:T(8,128)S(1)}, f32[1,4,48,96]{3,2,1,0:T(8,128)}, u32[]{:S(2)}) copy-start(f32[1,4,48,96]{3,2,1,0:T(8,128)} %param.29) | copy-start | bytes 221188
Sparse Core Ops, SparseCore 0:
  34.8 20.8 all-gather.4
  57.9 21.8 all-gather.6
  88.4 30.3 reduce-scatter.2
  152.4 66.6 reduce-scatter.4
where the time goes:
time: 228 us; the launch traced here: 227 us
  blocking collectives  102 us (45%)
  waiting for transfers between devices  40.6 us (18%)
  matrix products  39.3 us (17%)
  between operations  14.1 us (6%)
  other arithmetic  13 us (6%)
  local copies, waits for them, and re-layouts  11.9 us (5%)
  starting transfers between devices  5.85 us (3%)
    all_gather x2, blocking collectives, carried_in(): everything = jax.tree.map(lambda part: lax.all_gather(part, axis), x)  55.5 us
    all_to_all x1, blocking collectives, on_device(): lax.all_to_all(send_rows, 'sp', split_axis=0, concat_axis=0, tiled=True)  21.6 us
    all_gather x1, waiting for transfers between devices, on_device(): lax.all_gather(part_grad, 'tp', axis=1, tiled=True)  18 us
    all_to_all x1, blocking collectives, on_device(): lax.all_to_all(send_grad, 'sp', split_axis=0, concat_axis=0, tiled=True)  17.5 us
    reduce_scatter x1, waiting for transfers between devices, on_device(): lax.psum_scatter(lax.dot_general(stream, retained, along, preferred_eleme...  11.4 us
    select_n x8, other arithmetic, lap(): return jax.tree.map(lambda a, b: jnp.where(reached, a, b), new, before)  7.84 us
    all_gather x1, blocking collectives, on_device(): stream = lax.all_gather(stream_part, 'tp', axis=1, tiled=True)  7.66 us
    unnamed x44, local copies, waits for them, and re-layouts  5.57 us
  transfers between devices with their start and end apart: 5, of which 5 were waited for; matrix products, arithmetic and copies ran while one was open for 18% of the time, Pallas kernels for 0%

commit v1 on v0

v1 whole, which is shorter than its diff:
```python
import functools

import jax
import jax.numpy as jnp
from jax import lax
from jax.experimental import pallas as pl
from jax.experimental.pallas import tpu as pltpu
from jax.sharding import PartitionSpec as P


F32 = jnp.float32
BF16 = jnp.bfloat16
ACROSS = (((1,), (1,)), ((), ()))
ALONG = (((0,), (0,)), ((), ()))
CHUNKS = 2
START_VMEM = 60 << 20
WEIGHTS_VMEM = 52 << 20


def swap(x, axis, offset):
    count = lax.axis_size(axis)
    return lax.ppermute(x, axis, [(d, d ^ offset) for d in range(count)])


def powers(count):
    bits = []
    bit = 1
    while bit < count:
        bits.append(bit)
        bit *= 2
    return bits


def dot(a, b, dims=(((1,), (0,)), ((), ()))):
    return lax.dot_general(a, b, dims, preferred_element_type=F32)


def lanes(shape, head, per_head):
    lane = lax.broadcasted_iota(jnp.int32, shape, 1)
    return (lane >= head * per_head) & (lane < (head + 1) * per_head)


def spread_heads(columns, shape, per_head):
    out = jnp.zeros(shape, F32)
    for head in range(shape[1] // per_head):
        out = jnp.where(lanes(shape, head, per_head), columns[:, head : head + 1], out)
    return out


def masked(x, head, per_head):
    return jnp.where(lanes(x.shape, head, per_head), x, jnp.zeros_like(x))


def blocks_on_diagonal(packed, heads, value_dim):
    return jnp.concatenate([masked(packed, head, value_dim) for head in range(heads)], axis=0)


def start_kernel(tp_ref, sp_ref, *refs, slots, blocks, heads, key_dim, value_dim):
    sources, outs, scratch, arrivals = refs[:9], refs[9 : 17 + blocks], refs[17 + blocks : -1], refs[-1]
    send_refs, outs = outs[:blocks], outs[blocks:]
    columns = scratch[3].shape[1]
    start = pl.multiple_of(tp_ref[0] * columns, 128)
    copies = [
        pltpu.make_async_copy(
            source.at[:, pl.ds(start, columns)] if n == 2 else source, target, arrivals.at[n]
        )
        for n, (source, target) in enumerate(zip(sources, scratch))
    ]
    for copy in copies:
        copy.start()
    pick_part(copies, sp_ref, *scratch[:4], send_refs, outs[0], slots=slots, blocks=blocks)
    for copy in copies[4:]:
        copy.wait()
    prepare_part(*scratch[4:], *outs[1:], heads=heads, key_dim=key_dim, value_dim=value_dim)


def pick_part(copies, sp_ref, ids_ref, weights_ref, rows_ref, grad_ref, send_refs, pick_ref, *, slots, blocks):
    columns = grad_ref.shape[1]
    copies[0].wait()
    tokens = ids_ref.shape[1]
    total = slots * blocks
    first, second = ids_ref[0:1, :], ids_ref[1:2, :]
    expert = lax.broadcasted_iota(jnp.int32, (-(-blocks // 16) * 16, tokens), 0)
    one, two = expert == first, expert == second
    both = jnp.where(one | two, 1.0, 0.0).astype(BF16)
    row = lax.broadcasted_iota(jnp.int32, (tokens, tokens), 0)
    col = lax.broadcasted_iota(jnp.int32, (tokens, tokens), 1)
    count = dot(both, jnp.where(row < col, 1.0, 0.0).astype(BF16))
    rank_one = jnp.sum(jnp.where(one, count, 0.0), axis=0, keepdims=True)
    rank_two = jnp.sum(jnp.where(two, count, 0.0), axis=0, keepdims=True)

    slot_one = (first ^ sp_ref[0]) * slots + rank_one.astype(jnp.int32)
    slot_two = (second ^ sp_ref[0]) * slots + rank_two.astype(jnp.int32)
    position = lax.broadcasted_iota(jnp.int32, (total, tokens), 0)
    hit_one, hit_two = position == slot_one, position == slot_two
    pick = jnp.where(hit_one | hit_two, 1.0, 0.0).astype(BF16)
    copies[1].wait()
    weight = jnp.sum(
        jnp.where(hit_one, weights_ref[0:1, :], 0.0) + jnp.where(hit_two, weights_ref[1:2, :], 0.0),
        axis=1,
        keepdims=True,
    )
    copies[2].wait()
    rows = dot(pick, rows_ref[...]).astype(BF16)
    copies[3].wait()
    grad = (dot(pick, grad_ref[...]) * weight).astype(BF16)
    for k in range(blocks):
        send_refs[k][:, :columns] = rows[k * slots : (k + 1) * slots]
        send_refs[k][:, columns:] = grad[k * slots : (k + 1) * slots]
    diagonal = row == col

    def as_column(line):
        return jnp.sum(jnp.where(diagonal, line, jnp.zeros_like(line)), axis=1, keepdims=True)

    place = lax.broadcasted_iota(jnp.int32, (tokens, total), 1)
    found = (place == as_column(slot_one)) | (place == as_column(slot_two))
    pick_ref[...] = jnp.where(found, 1.0, 0.0).astype(BF16)


def three_terms(x):
    high = x.astype(BF16)
    rest = x - high.astype(F32)
    middle = rest.astype(BF16)
    return high, middle, (rest - middle.astype(F32)).astype(BF16)


def prepare_part(log_ref, q_ref, k_ref, state_ref, kept_ref, decay_ref, decay_t_ref, scores_t_ref, qe_ref, sum_ref, incoming_ref, wide_ref, *, heads, key_dim, value_dim):
    tokens = q_ref.shape[0]
    row = lax.broadcasted_iota(jnp.int32, (tokens, tokens), 0)
    col = lax.broadcasted_iota(jnp.int32, (tokens, tokens), 1)
    below = jnp.where(col <= row, 1.0, 0.0).astype(BF16)
    terms = three_terms(log_ref[...])
    sums = sum([dot(below, term, ACROSS) for term in terms])
    flats = sum([dot(term, below, ACROSS) for term in terms])
    sum_ref[...] = sums[:, :heads]
    q, k = q_ref[...], k_ref[...]
    for head in range(heads):
        down = sums[:, head : head + 1]
        flat = flats[head : head + 1, :]
        decay = jnp.where(row >= col, jnp.exp(jnp.minimum(down - flat, 0.0)), 0.0)
        decay_t = jnp.where(col >= row, jnp.exp(jnp.minimum(flat - down, 0.0)), 0.0)
        decay_ref[head] = decay
        decay_t_ref[head] = decay_t
        scores_t_ref[head] = (dot(masked(k, head, key_dim), q, ACROSS) * decay_t).astype(BF16)
    qe_ref[...] = (q.astype(F32) * spread_heads(jnp.exp(sums), q.shape, key_dim)).astype(BF16)
    width = heads * value_dim
    from_lane = lax.broadcasted_iota(jnp.int32, (value_dim, width), 0)
    to_lane = lax.broadcasted_iota(jnp.int32, (value_dim, width), 1)
    for head in range(heads):
        put = jnp.where(to_lane == from_lane + head * value_dim, 1.0, 0.0).astype(BF16)
        incoming_ref[head * key_dim : (head + 1) * key_dim, :] = dot(
            state_ref[head].astype(BF16), put
        ).astype(BF16)
    last = spread_heads(sums[tokens - 8 : tokens], (8, width), value_dim)[7:8]
    high, middle, low = three_terms(last)
    line = lax.broadcasted_iota(jnp.int32, (16, width), 0)
    extra = jnp.where(line == 0, high.astype(F32), 0.0)
    extra = jnp.where(line == 1, middle.astype(F32), extra)
    extra = jnp.where(line == 2, low.astype(F32), extra)
    extra = extra.astype(BF16)
    kept = kept_ref[...]
    for block in range(wide_ref.shape[0]):
        wide_ref[block, :tokens, :] = kept
        wide_ref[block, tokens:, :] = extra


def order_kernel(tp_ref, sp_ref, wide_ref, last_ref, own_ref, other_ref, sums_ref, *, turn):
    kept, rows, _ = wide_ref.shape
    half = (rows - 16) // 2
    own = pl.multiple_of((tp_ref[0] & 1) * half, 16)
    for position in range(2 * kept):
        offset = sum(bit for step, bit in enumerate(turn) if position >> step & 1)
        ref, at = (wide_ref, position) if position < kept else (last_ref, position - kept)
        block = sp_ref[0] ^ offset
        target = pl.ds(pl.multiple_of(block * half, 16), half)
        own_ref[target, :] = ref[at, pl.ds(own, half), :]
        other_ref[target, :] = ref[at, pl.ds(half - own, half), :]
        tail = ref[at, 2 * half :, :].astype(F32)
        sums_ref[pl.ds(block, 1), :] = tail[0:1] + tail[1:2] + tail[2:3]


def pair_kernel(sp_ref, sums_ref, added_ref, partner_ref, pair_ref):
    odd = (sp_ref[0] & 1) == 1
    added, partner = added_ref[...].astype(F32), partner_ref[...].astype(F32)
    first, second = jnp.where(odd, partner, added), jnp.where(odd, added, partner)
    decay = jnp.exp(sums_ref[pl.ds(sp_ref[0] & ~1, 1), :])
    pair_ref[...] = (first + decay * second).astype(BF16)


def inject_kernel(stream_ref, proj_ref, qe_ref, o_ref, inject_ref, *, heads, key_dim, value_dim):
    o = dot(stream_ref[...], proj_ref[...], ACROSS).astype(BF16)
    o_ref[...] = o
    cross = dot(qe_ref[...], o, ALONG)
    packed = jnp.zeros((key_dim, heads * value_dim), F32)
    for head in range(heads):
        packed = packed + masked(cross[head * key_dim : (head + 1) * key_dim], head, value_dim)
    inject_ref[...] = packed.astype(BF16)


def inner_kernel(o_ref, v_ref, q_ref, k_ref, decay_ref, decay_t_ref, scores_t_ref, sum_ref, state_ref, query_ref, key_ref, value_ref, *, heads, key_dim, value_dim):
    o, v, q, k = o_ref[...], v_ref[...], q_ref[...], k_ref[...]
    growth = spread_heads(jnp.exp(sum_ref[...]), q.shape, key_dim)
    query = growth * dot(o, state_ref[...], ACROSS)
    key = jnp.zeros(k.shape, F32)
    value = jnp.zeros(v.shape, F32)
    for head in range(heads):
        o_head = masked(o, head, value_dim)
        prob = (dot(o_head, v, ACROSS) * decay_ref[head]).astype(BF16)
        prob_t = (dot(v, o_head, ACROSS) * decay_t_ref[head]).astype(BF16)
        query = query + dot(prob, masked(k, head, key_dim))
        key = key + dot(prob_t, masked(q, head, key_dim))
        value = value + dot(scores_t_ref[head], o_head)
    query_ref[...] = query.astype(BF16)
    key_ref[...] = key
    value_ref[...] = value


def outer_kernel(sp_ref, blocks_ref, sum_ref, k_ref, v_ref, key_in_ref, value_in_ref, *refs, heads, key_dim, value_dim):
    k, v = k_ref[...], v_ref[...]
    *arrived, key_ref, value_ref = refs
    state = jnp.zeros(arrived[0].shape, F32)
    here = sp_ref[0]
    for at, arrived_ref in enumerate(arrived):
        source = here ^ 1 if at == 0 else (here ^ (2 * at)) & ~1
        total = jnp.zeros((1, state.shape[1]), F32)
        for block in range(blocks_ref.shape[0]):
            between = (block > here) & (block < source)
            total = total + jnp.where(between, blocks_ref[block : block + 1, :], 0.0)
        state = state + arrived_ref[...].astype(F32) * jnp.where(source > here, jnp.exp(total), 0.0)
    state = blocks_on_diagonal(state, heads, value_dim).astype(BF16)
    sums = sum_ref[...]
    tail = jnp.exp(sums[sums.shape[0] - 1 :, :] - sums)
    key_ref[...] = (
        key_in_ref[...] + spread_heads(tail, k.shape, key_dim) * dot(v, state, ACROSS)
    ).astype(BF16)
    value_ref[...] = (
        value_in_ref[...] + spread_heads(tail, v.shape, value_dim) * dot(k, state)
    ).astype(BF16)


def weights_kernel(at_ref, gate_ref, up_ref, down_ref, mine_in, other_in, mine_down, other_down, arrivals, *, even, columns):
    hidden = gate_ref.shape[1]
    copies = []
    for low, (into, down) in enumerate(((mine_in, mine_down), (other_in, other_down))):
        for position, at in enumerate(even):
            source = pl.ds(pl.multiple_of((at_ref[0] ^ (at ^ low)) * columns, 128), columns)
            target = pl.ds(position * columns, columns)
            for from_ref, to_ref in (
                (gate_ref.at[source, :], into.at[target, pl.ds(0, hidden)]),
                (up_ref.at[source, :], into.at[target, pl.ds(hidden, hidden)]),
                (down_ref.at[:, source], down.at[:, target]),
            ):
                copies.append(pltpu.make_async_copy(from_ref, to_ref, arrivals.at[len(copies)]))
                copies[-1].start()
    for copy in copies:
        copy.wait()


def chosen(mine, other):
    return jnp.where(pl.program_id(1) == 0, mine[...], other[...])


def down_kernel(at_ref, *refs):
    acts, mine, other, out = refs[:CHUNKS], refs[CHUNKS : 2 * CHUNKS], refs[2 * CHUNKS : 3 * CHUNKS], refs[-1]
    total = sum([dot(act[...], chosen(m, o), ALONG) for act, m, o in zip(acts, mine, other)])
    out[...] = total.astype(BF16)


def into_kernel(at_ref, *refs):
    gates, ups, mine, other = [refs[n * CHUNKS : (n + 1) * CHUNKS] for n in range(4)]
    pieces = [chosen(m, o) for m, o in zip(mine, other)]
    for grads, out in ((gates, refs[-2]), (ups, refs[-1])):
        out[...] = sum([dot(p, g[...], ALONG) for p, g in zip(pieces, grads)]).astype(BF16)


def stream_kernel(at_ref, mine_ref, other_ref, stream_ref, send_ref, *, even, columns):
    _, half, out_columns = send_ref.shape
    per_piece = columns // out_columns
    row = pl.multiple_of((at_ref[0] & 1) * half, 16)
    for low, ref in enumerate((mine_ref, other_ref)):
        for position, at in enumerate(even):
            place = at_ref[0] ^ (at ^ low)
            span = pl.ds(position * columns, columns)
            stream_ref[:, pl.ds(pl.multiple_of(place * columns, 128), columns)] = ref[:, span]
            for b in range(per_piece):
                send_ref[place * per_piece + b] = ref[
                    pl.ds(row, half), pl.ds(position * columns + b * out_columns, out_columns)
                ]


def assemble_kernel(*refs):
    *pieces, rows_ref, grad_ref = refs
    columns = pieces[0].shape[1] // 2
    across = rows_ref.shape[1] // columns
    slots = pieces[0].shape[0]
    for n, piece in enumerate(pieces):
        block = pl.ds(n // across * slots, slots)
        span = pl.ds(n % across * columns, columns)
        rows_ref[block, span] = piece[:, :columns]
        grad_ref[block, span] = piece[:, columns:]


def shaped(shape, dtype):
    return jax.ShapeDtypeStruct(shape, dtype)


def call(kernel, out_shape, flops, *args, megabytes=12, **settings):
    return pl.pallas_call(
        functools.partial(kernel, **settings) if settings else kernel,
        in_specs=[
            pl.BlockSpec(memory_space=pltpu.SMEM if arg.dtype == jnp.int32 and arg.ndim == 1 else pltpu.VMEM)
            for arg in args
        ],
        out_specs=jax.tree.map(lambda _: pl.BlockSpec(memory_space=pltpu.VMEM), out_shape),
        out_shape=out_shape,
        compiler_params=pltpu.CompilerParams(vmem_limit_bytes=megabytes << 20),
        cost_estimate=pl.CostEstimate(flops=flops, bytes_accessed=1 << 20, transcendentals=0),
    )(*args)


def on_device(
    moe_input,
    out_grad,
    expert_ids,
    expert_weights,
    w_gate,
    w_up,
    w_down,
    out_proj,
    retained,
    queries,
    keys,
    values,
    log_decay,
    incoming_state,
):
    tokens_here, width = moe_input.shape
    sp_count = lax.axis_size("sp")
    tp_count = lax.axis_size("tp")
    sp_at = lax.axis_index("sp")
    tp_at = lax.axis_index("tp")
    tp_bits = powers(tp_count)
    far_bits = tp_bits[:0:-1]
    capacity = 5 * tokens_here // (2 * sp_count)
    slots = -(-capacity // 16) * 16
    slot_count = sp_count * slots
    columns = width // tp_count
    heads = log_decay.shape[1]
    key_width, value_width = queries.shape[1], values.shape[1]
    key_dim, value_dim = key_width // heads, value_width // heads
    hidden = w_gate.shape[2]

    hbm = pl.BlockSpec(memory_space=pltpu.HBM)
    vmem = pl.BlockSpec(memory_space=pltpu.VMEM)
    smem = pl.BlockSpec(memory_space=pltpu.SMEM)
    even = [0]
    for bit in far_bits:
        even = even + [at ^ bit for at in even]

    log_rows = log_decay.T
    if heads == 1:
        log_rows = jnp.pad(log_rows, ((0, 7), (0, 0)))
    square = (heads, tokens_here, tokens_here)
    sources = (
        expert_ids.T,
        expert_weights.T,
        moe_input,
        out_grad,
        log_rows,
        queries,
        keys,
        incoming_state[0],
        retained,
    )
    held = [shaped((tokens_here, columns) if n == 2 else x.shape, x.dtype) for n, x in enumerate(sources)]
    plain = pl.BlockSpec(memory_space=None)
    into = shaped((len(even) * columns, 2 * hidden), BF16)
    down = shaped((hidden, len(even) * columns), BF16)
    (
        *to_send,
        picker,
        decay,
        decay_t,
        scores_t,
        grown,
        running_total,
        incoming,
        wide,
    ) = pl.pallas_call(
        functools.partial(
            start_kernel, slots=slots, blocks=sp_count, heads=heads, key_dim=key_dim, value_dim=value_dim
        ),
        in_specs=[smem, smem] + [hbm] * len(sources),
        out_specs=[vmem] * sp_count + [plain] * 8,
        out_shape=[shaped((slots, 2 * columns), BF16)] * sp_count
        + [
            shaped((tokens_here, slot_count), BF16),
            shaped(square, F32),
            shaped(square, F32),
            shaped(square, BF16),
            shaped(queries.shape, BF16),
            shaped(log_decay.shape, F32),
            shaped((key_width, value_width), BF16),
            shaped((1, tokens_here + 16, value_width), BF16),
        ],
        scratch_shapes=[pltpu.VMEM(x.shape, x.dtype) for x in held] + [pltpu.SemaphoreType.DMA((len(held),))],
        compiler_params=pltpu.CompilerParams(vmem_limit_bytes=START_VMEM),
        cost_estimate=pl.CostEstimate(
            flops=4 * slot_count * tokens_here * columns, bytes_accessed=1 << 20, transcendentals=0
        ),
        name="start",
    )(tp_at.reshape(1), sp_at.reshape(1), *sources)

    def near(x):
        return swap(x, "tp", 1)

    def block_of(x, k):
        return x[k * slots : (k + 1) * slots]

    parts = [to_send[0]]
    for k in range(1, sp_count):
        parts.append(swap(to_send[k], "sp", k))

    def far_pieces(x):
        pieces = [x]
        for bit in far_bits:
            pieces = pieces + [swap(piece, "tp", bit) for piece in pieces]
        return pieces

    mine_in, other_in, mine_down, other_down = pl.pallas_call(
        functools.partial(weights_kernel, even=even, columns=columns),
        in_specs=[smem, hbm, hbm, hbm],
        out_specs=[vmem] * 4,
        out_shape=[into, into, down, down],
        scratch_shapes=[pltpu.SemaphoreType.DMA((3 * tp_count,))],
        compiler_params=pltpu.CompilerParams(vmem_limit_bytes=WEIGHTS_VMEM),
        cost_estimate=pl.CostEstimate(flops=1 << 30, bytes_accessed=1 << 20, transcendentals=0),
        name="weights",
    )(tp_at.reshape(1), w_gate[0], w_up[0], w_down[0])

    gathered = [far_pieces(x) for x in parts]
    per_chunk = sp_count // CHUNKS
    rows_mine, rows_other, grad_mine, grad_other = [], [], [], []
    for c in range(CHUNKS):
        of_chunk = [piece for k in range(c * per_chunk, (c + 1) * per_chunk) for piece in gathered[k]]
        joined = shaped((per_chunk * slots, len(even) * columns), BF16)
        whole = call(assemble_kernel, [joined, joined], 1 << 28, *of_chunk)
        rows_mine.append(whole[0])
        grad_mine.append(whole[1])
        rows_other.append(near(whole[0]))
        grad_other.append(near(whole[1]))

    acts, gate_grads, up_grads, returned = [], [], [], []
    for c in range(CHUNKS):
        both = dot(rows_mine[c], mine_in) + dot(rows_other[c], other_in)
        gate, up = both[:, :hidden], both[:, hidden:]
        sig = jax.nn.sigmoid(gate)
        swish = gate * sig
        acts.append((swish * up).astype(BF16))
        act_grad = dot(grad_mine[c], mine_down, ACROSS) + dot(grad_other[c], other_down, ACROSS)
        gate_grad = (act_grad * up * sig * (1.0 + gate * (1.0 - sig))).astype(BF16)
        up_grad = (act_grad * swish).astype(BF16)
        gate_grads.append(gate_grad)
        up_grads.append(up_grad)
        both_grad = jnp.concatenate([gate_grad, up_grad], axis=1)
        arrived = near(dot(both_grad, other_in, ACROSS).astype(BF16))
        sums = {}
        for position, at in reversed(list(enumerate(even))):
            span = slice(position * columns, (position + 1) * columns)
            sums[at] = dot(both_grad, mine_in[span], ACROSS) + arrived[:, span].astype(F32)
        for bit in tp_bits[1:]:
            sums = {
                at: sums[at] + swap(sums[at ^ bit].astype(BF16), "tp", bit).astype(F32)
                for at in sums
                if not at & bit
            }
        share = sums[0].astype(BF16)
        for k in range(per_chunk):
            block = block_of(share, k)
            at = c * per_chunk + k
            returned.append(swap(block, "sp", at) if at else block)

    places = jnp.asarray([at ^ low for at in even for low in (0, 1)], jnp.int32) ^ tp_at
    chunk_rows = per_chunk * slots
    narrow = pl.BlockSpec((chunk_rows, columns), lambda p, low, at: (0, p))
    fixed = pl.BlockSpec((chunk_rows, hidden), lambda p, low, at: (0, 0))
    by_row = pl.BlockSpec((columns, hidden), lambda p, low, at: (at[2 * p + low], 0))
    by_column = pl.BlockSpec((hidden, columns), lambda p, low, at: (0, at[2 * p + low]))

    def gradients(kernel, in_specs, out_specs, out_shape, *args):
        return pl.pallas_call(
            kernel,
            grid_spec=pltpu.PrefetchScalarGridSpec(
                num_scalar_prefetch=1, grid=(len(even), 2), in_specs=in_specs, out_specs=out_specs
            ),
            out_shape=out_shape,
            compiler_params=pltpu.CompilerParams(vmem_limit_bytes=16 << 20),
            cost_estimate=pl.CostEstimate(flops=1 << 32, bytes_accessed=1 << 20, transcendentals=0),
        )(places, *args)

    (down_grad,) = gradients(
        down_kernel,
        [fixed] * CHUNKS + [narrow] * (2 * CHUNKS),
        [by_column],
        [shaped((hidden, width), BF16)],
        *acts,
        *grad_mine,
        *grad_other,
    )
    gate_w_grad, up_w_grad = gradients(
        into_kernel,
        [fixed] * (2 * CHUNKS) + [narrow] * (2 * CHUNKS),
        [by_row, by_row],
        [shaped((width, hidden), BF16)] * 2,
        *gate_grads,
        *up_grads,
        *rows_mine,
        *rows_other,
    )

    token_grad = dot(picker, jnp.concatenate(returned, axis=0))
    stream_part = (out_grad.astype(F32) + token_grad).astype(BF16)
    stream_mine = jnp.concatenate(far_pieces(stream_part), axis=1)
    stream_other = near(stream_mine)
    half = tokens_here // 2
    out_columns = width // sp_count
    stream, columns_out = call(
        functools.partial(stream_kernel, even=even, columns=columns),
        [shaped((tokens_here, width), BF16), shaped((sp_count, half, out_columns), BF16)],
        1 << 28,
        tp_at.reshape(1),
        stream_mine,
        stream_other,
    )

    sp_bits = powers(sp_count)
    turn = sp_bits[1:] + sp_bits[:1]
    for bit in turn[:-1]:
        wide = jnp.concatenate([wide, swap(wide, "sp", bit)], axis=0)
    last = swap(wide, "sp", turn[-1])

    halves = shaped((sp_count * half, value_width), BF16)
    own_rows, other_rows, block_sums = call(
        functools.partial(order_kernel, turn=tuple(turn)),
        [halves, halves, shaped((sp_count, value_width), F32)],
        1 << 28,
        tp_at.reshape(1),
        sp_at.reshape(1),
        wide,
        last,
    )

    got_half = lax.all_to_all(columns_out, "sp", split_axis=0, concat_axis=0, tiled=True)
    other_half = near(got_half)
    own_cols = got_half.reshape(-1, out_columns)
    other_cols = other_half.reshape(-1, out_columns)
    own_part = dot(own_cols, own_rows, ALONG)
    out_proj_grad = own_part + dot(other_cols, other_rows, ALONG)

    sizes = dict(heads=heads, key_dim=key_dim, value_dim=value_dim)
    o, added = call(
        inject_kernel,
        [
            shaped((tokens_here, value_width), BF16),
            shaped((key_dim, value_width), BF16),
        ],
        1 << 30,
        stream,
        out_proj,
        grown,
        **sizes,
    )
    partner = swap(added, "sp", 1)
    pair = call(pair_kernel, shaped(added.shape, BF16), 1 << 26, sp_at.reshape(1), block_sums, added, partner)
    arrived = [partner]
    for k in range(2, sp_count, 2):
        arrived.append(swap(pair, "sp", k))

    query_grad, key_inner, value_inner = call(
        inner_kernel,
        [shaped(queries.shape, BF16), shaped(keys.shape, F32), shaped(values.shape, F32)],
        1 << 32,
        o,
        values,
        queries,
        keys,
        decay,
        decay_t,
        scores_t,
        running_total,
        incoming,
        **sizes,
    )

    key_grad, value_grad = call(
        outer_kernel,
        [shaped(keys.shape, BF16), shaped(values.shape, BF16)],
        1 << 30,
        sp_at.reshape(1),
        block_sums,
        running_total,
        keys,
        values,
        key_inner,
        value_inner,
        *arrived,
        **sizes,
    )
    return (
        gate_w_grad[None],
        up_w_grad[None],
        down_grad[None],
        out_proj_grad,
        query_grad,
        key_grad,
        value_grad,
    )


def solution(mesh):
    placed = (
        P("sp", None),
        P("sp", "tp"),
        P("sp", None),
        P("sp", None),
        P("sp", None, "tp"),
        P("sp", None, "tp"),
        P("sp", "tp", None),
        P("tp", None),
        P("sp", "tp"),
        P("sp", "tp"),
        P("sp", "tp"),
        P("sp", "tp"),
        P("sp", "tp"),
        P("sp", "tp", None, None),
    )

    return jax.shard_map(
        on_device,
        mesh=mesh,
        in_specs=placed,
        out_specs=(
            P("sp", None, "tp"),
            P("sp", None, "tp"),
            P("sp", "tp", None),
            P("sp", "tp"),
            P("sp", "tp"),
            P("sp", "tp"),
            P("sp", "tp"),
        ),
        check_vma=False,
    )
```

time: 228 us -> 156 us (0.68)
  blocking collectives: 102 us -> 0 us
  starting transfers between devices: 5.85 us -> 52.8 us
  matrix products: 39.3 us -> 14.8 us
  Pallas kernels: 0 us -> 21.9 us
  between operations: 14.1 us -> 1.3 us
  other arithmetic: 13 us -> 0.34 us
  waiting for transfers between devices: 40.6 us -> 51.6 us
    all_gather x3 -> x0, blocking collectives: 63.2 us -> none  [the longest x2 55.5 us: carried_in(): everything = jax.tree.map(lambda part: lax.all_gather(part, axis), x)]
    ppermute x0 -> x40, waiting for transfers between devices: none -> 51.6 us  [swap(): return lax.ppermute(x, axis, [(d, d ^ offset) for d in range(count)])]
    ppermute x0 -> x40, starting transfers between devices: none -> 48.4 us  [swap(): return lax.ppermute(x, axis, [(d, d ^ offset) for d in range(count)])]
    all_to_all x2 -> x0, blocking collectives: 39.1 us -> none  [the longest x1 21.6 us: on_device(): lax.all_to_all(send_rows, 'sp', split_axis=0, concat_axis=0, tiled=True)]
    dot_general x22 -> x17, matrix products: 39.3 us -> 14.8 us  [dot(): return lax.dot_general(a, b, dims, preferred_element_type=F32)]
    pallas_call x0 -> x12, Pallas kernels: none -> 21.9 us  [the longest x2 8.4 us: gradients(): pl.pallas_call(kernel, grid_spec=pltpu.PrefetchScalarGridSpec(num_scalar_...]
    all_gather x2 -> x0, waiting for transfers between devices: 19.6 us -> none  [the longest x1 18 us: on_device(): lax.all_gather(part_grad, 'tp', axis=1, tiled=True)]
    reduce_scatter x2 -> x0, waiting for transfers between devices: 16.6 us -> none  [the longest x1 11.4 us: on_device(): lax.psum_scatter(lax.dot_general(stream, retained, along, preferred_eleme...]
  transfers between devices with their start and end apart: 5 -> 41, of which waited for: 5 -> 17; matrix products, arithmetic and copies ran while one was open for 18% -> 8% of each run, Pallas kernels for 0% -> 11%
where the time goes in v1:
time: 156 us
  starting transfers between devices  52.8 us (34%)
  waiting for transfers between devices  51.6 us (33%)
  Pallas kernels  21.9 us (14%)
  matrix products  14.8 us (9%)
  local copies, waits for them, and re-layouts  12.7 us (8%)
    ppermute x40, waiting for transfers between devices, swap(): return lax.ppermute(x, axis, [(d, d ^ offset) for d in range(count)])  51.6 us
    ppermute x40, starting transfers between devices, swap(): return lax.ppermute(x, axis, [(d, d ^ offset) for d in range(count)])  48.4 us
    dot_general x17, matrix products, dot(): return lax.dot_general(a, b, dims, preferred_element_type=F32)  14.8 us
    unnamed x92, local copies, waits for them, and re-layouts  12.6 us
    pallas_call x2, Pallas kernels, gradients(): pl.pallas_call(kernel, grid_spec=pltpu.PrefetchScalarGridSpec(num_scalar_...  8.4 us
    pallas_call x1, Pallas kernels, on_device(): pl.pallas_call(functools.partial(weights_kernel, even=even, columns=colum...  5.28 us
    all_to_all x1, starting transfers between devices, on_device(): lax.all_to_all(columns_out, 'sp', split_axis=0, concat_axis=0, tiled=True)  4.41 us
    pallas_call x8, Pallas kernels, call(): pl.pallas_call(functools.partial(kernel, **settings) if settings else ker...  4.25 us
  transfers between devices with their start and end apart: 41, of which 17 were waited for; matrix products, arithmetic and copies ran while one was open for 8% of the time, Pallas kernels for 11%

profile of v1, /device:TPU:0, one launch (start us, length us, event | category | flops | bytes accessed | tf_op | source)
XLA Modules:
  0.0 155.5 jit_solution(535970978959414722)
XLA Ops:
  0.6 3.9 %start.1 = (bf16[64,1024]{1,0:T(8,128)(2,1)}, bf16[64,1024]{1,0:T(8,128)(2,1)}, bf16[64,1024]{1,0:T(8,128)(2,1)}, bf16[64,1024]{1,0:T(8,128)(2,1)}, bf16[64,1024...) custom-call(s32[1]{0:T(128)} %bitcast.tp_ref.at_ref, ...), custom_call_target="tpu_custom_call" | custom-call | flops 201326592 | bytes 1048576 | tf_op jit(solution)/shard_map/start/pallas_call | solution.py:389
  4.6 4.1 %collective-permute-start.9 = (bf16[64,1024]{1,0:T(8,128)(2,1)}, bf16[64,1024]{1,0:T(8,128)(2,1)S(1)}, u32[]{:S(2)}, u32[]{:S(2)}) collective-permute-start(bf16[64,1024]{1,0:T(8,128)(2,1)} %get-tuple-element.55), channel_id=1, source_target_pairs={{0,16},{4,20},{8,24},{12,28},{16,0},{20,4},{24,8},{28,12},{1,17},{... | collective-permute-start | bytes 393224 | tf_op jit(solution)/shard_map/ppermute | solution.py:22
  10.0 3.6 %collective-permute-start.13 = (bf16[64,1024]{1,0:T(8,128)(2,1)}, bf16[64,1024]{1,0:T(8,128)(2,1)S(1)}, u32[]{:S(2)}, u32[]{:S(2)}) collective-permute-start(bf16[64,1024]{1,0:T(8,128)(2,1)} %get-tuple-element.57), channel_id=1, source_target_pairs={{0,24},{4,28},{8,16},{12,20},{16,8},{20,12},{24,0},{28,4},{1,25},{... | collective-permute-start | bytes 393224 | tf_op jit(solution)/shard_map/ppermute | solution.py:22
  13.6 10.9 %collective-permute-done.9.refs_0_ = bf16[64,1024]{1,0:T(8,128)(2,1)S(1)} collective-permute-done((bf16[64,1024]{1,0:T(8,128)(2,1)}, bf16[64,1024]{1,0:T(8,128)(2,1)S(1)}, u32[]{:S(2)}, u32[]{:S(2)}) %collective-permute-start.9) | collective-permute-done | bytes 131104 | tf_op jit(solution)/shard_map/ppermute | solution.py:22
  24.5 1.8 %collective-permute-start.10 = (bf16[64,1024]{1,0:T(8,128)(2,1)S(1)}, bf16[64,1024]{1,0:T(8,128)(2,1)S(1)}, u32[]{:S(2)}, u32[]{:S(2)}) collective-permute-start(bf16[64,1024]{1,0:T(8,128)(2,1)S(1)} %collective-permute-done.9.refs_0_), channel_id=1, source_target_pairs={{0,2},{1,3},{2,0},{3,1},{4,6},{5,7},{6,4},{7,5},{8,10},{9,11},{10,... | collective-permute-start | bytes 393224 | tf_op jit(solution)/shard_map/ppermute | solution.py:22
  26.3 2.2 %collective-permute-done.11.refs_2_ = bf16[64,1024]{1,0:T(8,128)(2,1)S(1)} collective-permute-done((bf16[64,1024]{1,0:T(8,128)(2,1)}, bf16[64,1024]{1,0:T(8,128)(2,1)S(1)}, u32[]{:S(2)}, u32[]{:S(2)}) %collective-permute-start.11) | collective-permute-done | bytes 131104 | tf_op jit(solution)/shard_map/ppermute | solution.py:22
  30.6 1.5 collective-permute-start.16
  32.1 2.8 %collective-permute-done.12.refs_3_ = bf16[64,1024]{1,0:T(8,128)(2,1)S(1)} collective-permute-done((bf16[64,1024]{1,0:T(8,128)(2,1)S(1)}, bf16[64,1024]{1,0:T(8,128)(2,1)S(1)}, u32[]{:S(2)}, u32[]{:S(2)}) %collective-permute-start.12) | collective-permute-done | bytes 131104 | tf_op jit(solution)/shard_map/ppermute | solution.py:22
  34.9 1.6 %collective-permute-done.14.refs_5_ = bf16[64,1024]{1,0:T(8,128)(2,1)S(1)} collective-permute-done((bf16[64,1024]{1,0:T(8,128)(2,1)S(1)}, bf16[64,1024]{1,0:T(8,128)(2,1)S(1)}, u32[]{:S(2)}, u32[]{:S(2)}) %collective-permute-start.14) | collective-permute-done | bytes 131104 | tf_op jit(solution)/shard_map/ppermute | solution.py:22
  38.1 1.8 %collective-permute-start.1 = (bf16[64,1024]{1,0:T(8,128)(2,1)}, bf16[64,1024]{1,0:T(8,128)(2,1)S(1)}, u32[]{:S(2)}, u32[]{:S(2)}) collective-permute-start(bf16[64,1024]{1,0:T(8,128)(2,1)} %get-tuple-element.46), channel_id=1, source_target_pairs={{0,4},{4,0},{8,12},{12,8},{16,20},{20,16},{24,28},{28,24},{1,5},{5... | collective-permute-start | bytes 393224 | tf_op jit(solution)/shard_map/ppermute | solution.py:22
  41.6 1.8 %collective-permute-start = (bf16[64,1024]{1,0:T(8,128)(2,1)}, bf16[64,1024]{1,0:T(8,128)(2,1)S(1)}, u32[]{:S(2)}, u32[]{:S(2)}) collective-permute-start(bf16[64,1024]{1,0:T(8,128)(2,1)} %get-tuple-element.45.refs_0_), channel_id=1, source_target_pairs={{0,2},{1,3},{2,0},{3,1},{4,6},{5,7},{6,4},{7,5},{8,10},{9,11},{10,... | collective-permute-start | bytes 393224 | tf_op jit(solution)/shard_map/ppermute | solution.py:22
  44.2 1.8 %collective-permute-start.2 = (bf16[64,1024]{1,0:T(8,128)(2,1)S(1)}, bf16[64,1024]{1,0:T(8,128)(2,1)S(1)}, u32[]{:S(2)}, u32[]{:S(2)}) collective-permute-start(bf16[64,1024]{1,0:T(8,128)(2,1)S(1)} %collective-permute-done.1.refs_2_), channel_id=1, source_target_pairs={{0,2},{1,3},{2,0},{3,1},{4,6},{5,7},{6,4},{7,5},{8,10},{9,11},{10,... | collective-permute-start | bytes 393224 | tf_op jit(solution)/shard_map/ppermute | solution.py:22
  48.2 1.8 %collective-permute-start.6 = (bf16[64,1024]{1,0:T(8,128)(2,1)S(1)}, bf16[64,1024]{1,0:T(8,128)(2,1)S(1)}, u32[]{:S(2)}, u32[]{:S(2)}) collective-permute-start(bf16[64,1024]{1,0:T(8,128)(2,1)S(1)} %collective-permute-done.5.refs_6_), channel_id=1, source_target_pairs={{0,2},{1,3},{2,0},{3,1},{4,6},{5,7},{6,4},{7,5},{8,10},{9,11},{10,... | collective-permute-start | bytes 393224 | tf_op jit(solution)/shard_map/ppermute | solution.py:22
  50.0 5.3 %weights.1 = (bf16[1024,1024]{1,0:T(8,128)(2,1)}, bf16[1024,1024]{1,0:T(8,128)(2,1)}, bf16[512,1024]{1,0:T(8,128)(2,1)S(1)}, bf16[512,1024]{1,0:T(8,128)(2,1)}) custom-call(s32[1]{0:T(128)} %bitcast.tp_ref.at_ref, bf16[2048,512]{1,0:T(8,128)(2,1)} %bitcast.38, bf16[2048,512]{1,0:T(8,128)(2,1)} %bitcast.39, bf16[512,2048]{1,0:T(8,128)(2,1)} %bitcast.40), custom_call_target="tpu_custom_call" | custom-call | flops 1073741824 | bytes 1048576 | tf_op jit(solution)/shard_map/weights/pallas_call | solution.py:430
  56.7 2.5 %fusion.26 = f32[256,1024]{1,0:T(8,128)S(1)} fusion(bf16[256,1024]{1,0:T(8,128)(2,1)S(1)} %collective-permute-done.18.refs_7_, bf16[1024,1024]{1,0:T(8,128)(2,1)} %get-tuple-element.54), kind=kOutput, calls=%fused_computation.58 | convolution fusion | flops 536870912 | bytes 3670016 | tf_op jit(solution)/shard_map/dot_general | solution.py:35
  74.1 6.5 %collective-permute-done.20 = bf16[256,512]{1,0:T(8,128)(2,1)S(1)} collective-permute-done((bf16[256,512]{1,0:T(8,128)(2,1)S(1)}, bf16[256,512]{1,0:T(8,128)(2,1)S(1)}, u32[]{:S(2)}, u32[]{:S(2)}) %collective-permute-start.20) | collective-permute-done | bytes 262176 | tf_op jit(solution)/shard_map/ppermute | solution.py:22
  80.8 1.6 %collective-permute-start.21 = (bf16[64,512]{1,0:T(8,128)(2,1)S(1)}, bf16[64,512]{1,0:T(8,128)(2,1)S(1)}, u32[]{:S(2)}, u32[]{:S(2)}) collective-permute-start(bf16[64,512]{1,0:T(8,128)(2,1)S(1)} %get-tuple-element.95), channel_id=1, source_target_pairs={{0,4},{4,0},{8,12},{12,8},{16,20},{20,16},{24,28},{28,24},{1,5},{5... | collective-permute-start | bytes 196616 | tf_op jit(solution)/shard_map/ppermute | solution.py:22
  82.3 3.1 %collective-permute-done.25 = bf16[256,512]{1,0:T(8,128)(2,1)S(1)} collective-permute-done((bf16[256,512]{1,0:T(8,128)(2,1)S(1)}, bf16[256,512]{1,0:T(8,128)(2,1)S(1)}, u32[]{:S(2)}, u32[]{:S(2)}) %collective-permute-start.25) | collective-permute-done | bytes 262176 | tf_op jit(solution)/shard_map/ppermute | solution.py:22
  85.6 3.8 %collective-permute-start.26 = (bf16[64,512]{1,0:T(8,128)(2,1)S(1)}, bf16[64,512]{1,0:T(8,128)(2,1)S(1)}, u32[]{:S(2)}, u32[]{:S(2)}) collective-permute-start(bf16[64,512]{1,0:T(8,128)(2,1)S(1)} %get-tuple-element.92), channel_id=1, source_target_pairs={{0,16},{4,20},{8,24},{12,28},{16,0},{20,4},{24,8},{28,12},{1,17},{... | collective-permute-start | bytes 196616 | tf_op jit(solution)/shard_map/ppermute | solution.py:22
  93.7 1.7 %collective-permute-start.28 = (bf16[64,512]{1,0:T(8,128)(2,1)S(1)}, bf16[64,512]{1,0:T(8,128)(2,1)S(1)}, u32[]{:S(2)}, u32[]{:S(2)}) collective-permute-start(bf16[64,512]{1,0:T(8,128)(2,1)S(1)} %get-tuple-element.90), channel_id=1, source_target_pairs={{0,24},{4,28},{8,16},{12,20},{16,8},{20,12},{24,0},{28,4},{1,25},{... | collective-permute-start | bytes 196616 | tf_op jit(solution)/shard_map/ppermute | solution.py:22
  95.7 2.0 %collective-permute-start.29 = (bf16[64,512]{1,0:T(8,128)(2,1)S(1)}, bf16[64,512]{1,0:T(8,128)(2,1)S(1)}, u32[]{:S(2)}, u32[]{:S(2)}) collective-permute-start(bf16[64,512]{1,0:T(8,128)(2,1)S(1)} %get-tuple-element.89), channel_id=1, source_target_pairs={{0,28},{4,24},{8,20},{12,16},{16,12},{20,8},{24,4},{28,0},{1,29},{... | collective-permute-start | bytes 196616 | tf_op jit(solution)/shard_map/ppermute | solution.py:22
  97.7 3.0 %collective-permute-done.27 = bf16[64,512]{1,0:T(8,128)(2,1)S(1)} collective-permute-done((bf16[64,512]{1,0:T(8,128)(2,1)S(1)}, bf16[64,512]{1,0:T(8,128)(2,1)S(1)}, u32[]{:S(2)}, u32[]{:S(2)}) %collective-permute-start.27) | collective-permute-done | bytes 65568 | tf_op jit(solution)/shard_map/ppermute | solution.py:22
  100.7 2.1 %collective-permute-done.29 = bf16[64,512]{1,0:T(8,128)(2,1)S(1)} collective-permute-done((bf16[64,512]{1,0:T(8,128)(2,1)S(1)}, bf16[64,512]{1,0:T(8,128)(2,1)S(1)}, u32[]{:S(2)}, u32[]{:S(2)}) %collective-permute-start.29) | collective-permute-done | bytes 65568 | tf_op jit(solution)/shard_map/ppermute | solution.py:22
  103.9 4.9 %collective-permute-done.30 = bf16[192,512]{1,0:T(8,128)(2,1)S(1)} collective-permute-done((bf16[192,512]{1,0:T(8,128)(2,1)S(1)}, bf16[192,512]{1,0:T(8,128)(2,1)S(1)}, u32[]{:S(2)}, u32[]{:S(2)}) %collective-permute-start.30) | collective-permute-done | bytes 196640 | tf_op jit(solution)/shard_map/ppermute | solution.py:22
  109.2 9.0 %collective-permute-done.33 = bf16[2,208,384]{2,1,0:T(8,128)(2,1)S(1)} collective-permute-done((bf16[2,208,384]{2,1,0:T(8,128)(2,1)S(1)}, bf16[2,208,384]{2,1,0:T(8,128)(2,1)S(1)}, u32[]{:S(2)}, u32[]{:S(2)}) %collective-permute-start.33) | collective-permute-done | bytes 319520 | tf_op jit(solution)/shard_map/ppermute | solution.py:22
  120.2 4.4 %all-to-all-start = ((bf16[8,96,256]{2,1,0:T(8,128)(2,1)}), bf16[8,96,256]{2,1,0:T(8,128)(2,1)}, u32[]{:S(2)}, u32[]{:S(2)}) async-start(bf16[8,96,256]{2,1,0:T(8,128)(2,1)} %copy-done.4), calls=%async_computation | async-start | bytes 786432 | tf_op jit(solution)/shard_map/all_to_all | solution.py:553
  128.4 4.6 %shard_map.200 = (bf16[2048,512]{1,0:T(8,128)(2,1)}, bf16[2048,512]{1,0:T(8,128)(2,1)}) custom-call(s32[4]{0:T(128)S(1)} %iota_xor_fusion.at_ref, bf16[256,512]{1,0:T(8,128)(2,1)S(1)} %copy-done.31, bf16[256,512]{1,0:T(8,128)(2,1)S(1)} %copy-done.27, bf16[256,512]{1,0:T(8,128)(2,1)S(1)} %copy-done.29, bf16[256,512]{1,0:T(8,128)(2,1)S(1)} %copy-done.25, ...), custom_call_target="tpu_custom_call" | custom-call | flops 4294967296 | bytes 1048576 | tf_op jit(solution)/shard_map/pallas_call | solution.py:491
  134.7 2.0 %collective-permute-start.36 = (bf16[48,384]{1,0:T(8,128)(2,1)S(1)}, bf16[48,384]{1,0:T(8,128)(2,1)S(1)}, u32[]{:S(2)}, u32[]{:S(2)}) collective-permute-start(bf16[48,384]{1,0:T(8,128)(2,1)S(1)} %get-tuple-element.80.added_ref), channel_id=1, source_target_pairs={{0,4},{4,0},{8,12},{12,8},{16,20},{20,16},{24,28},{28,24},{1,5},{5... | collective-permute-start | bytes 110600 | tf_op jit(solution)/shard_map/ppermute | solution.py:22
  136.8 3.8 %shard_map.201 = bf16[512,2048]{1,0:T(8,128)(2,1)} custom-call(s32[4]{0:T(128)S(1)} %iota_xor_fusion.at_ref, bf16[256,512]{1,0:T(8,128)(2,1)S(1)} %copy-done.35, bf16[256,512]{1,0:T(8,128)(2,1)S(1)} %copy-done.34, bf16[256,1024]{1,0:T(8,128)(2,1)S(1)} %copy-done.14, bf16[256,1024]{1,0:T(8,128)(2,1)S(1)} %copy-done.12, bf16[256,1024]{1,0:T(8,128)(2,1)S(1)} %copy-done.3, ...), custom_call_target="tpu_custom_call" | custom-call | flops 4294967296 | bytes 1048576 | tf_op jit(solution)/shard_map/pallas_call | solution.py:491
  142.9 2.4 %collective-permute-start.38 = (bf16[48,384]{1,0:T(8,128)(2,1)S(1)}, bf16[48,384]{1,0:T(8,128)(2,1)S(1)}, u32[]{:S(2)}, u32[]{:S(2)}) collective-permute-start(bf16[48,384]{1,0:T(8,128)(2,1)S(1)} %shard_map.206), channel_id=1, source_target_pairs={{0,16},{4,20},{8,24},{12,28},{16,0},{20,4},{24,8},{28,12},{1,17},{... | collective-permute-start | bytes 110600 | tf_op jit(solution)/shard_map/ppermute | solution.py:22
  150.0 1.9 %shard_map.205 = (bf16[192,192]{1,0:T(8,128)(2,1)}, f32[192,192]{1,0:T(8,128)S(1)}, f32[192,384]{1,0:T(8,128)S(1)}) custom-call(bf16[192,384]{1,0:T(8,128)(2,1)S(1)} %copy-done.33, bf16[192,384]{1,0:T(8,128)(2,1)S(1)} %copy-done.16, bf16[192,192]{1,0:T(8,128)(2,1)S(1)} %copy-done.6, bf16[192,192]{1,0:T(8,128)(2,1)S(1)} %copy-done.7, ...), custom_call_target="tpu_custom_call" | custom-call | flops 4294967296 | bytes 1048576 | tf_op jit(solution)/shard_map/pallas_call | solution.py:308
  153.4 2.1 %convolution_add_fusion.5 = f32[256,384]{1,0:T(8,128)} fusion(f32[256,384]{1,0:T(8,128)S(1)} %fusion.27, bf16[768,256]{1,0:T(8,128)(2,1)} %bitcast.12, bf16[768,384]{1,0:T(8,128)(2,1)S(1)} %get-tuple-element.66), kind=kOutput, calls=%fused_computation.7 | convolution fusion | flops 151093248 | bytes 1769472 | tf_op jit(solution)/shard_map/dot_general | solution.py:35
  (180 shorter events, 47.8 us)
Async XLA Ops:
  4.6 19.9 %collective-permute-start.9 = (bf16[64,1024]{1,0:T(8,128)(2,1)}, bf16[64,1024]{1,0:T(8,128)(2,1)S(1)}, u32[]{:S(2)}, u32[]{:S(2)}) collective-permute-start(bf16[64,1024]{1,0:T(8,128)(2,1)} %get-tuple-element.55), channel_id=1, source_target_pairs={{0,16},{4,20},{8,24},{12,28},{16,0},{20,4},{24,8},{28,12},{1,17},{... | collective-permute-start | bytes 393224 | tf_op jit(solution)/shard_map/ppermute | solution.py:22
  8.7 19.8 %collective-permute-start.11 = (bf16[64,1024]{1,0:T(8,128)(2,1)}, bf16[64,1024]{1,0:T(8,128)(2,1)S(1)}, u32[]{:S(2)}, u32[]{:S(2)}) collective-permute-start(bf16[64,1024]{1,0:T(8,128)(2,1)} %get-tuple-element.56), channel_id=1, source_target_pairs={{0,20},{4,16},{8,28},{12,24},{16,4},{20,0},{24,12},{28,8},{1,21},{... | collective-permute-start | bytes 393224 | tf_op jit(solution)/shard_map/ppermute | solution.py:22
  10.0 20.1 %collective-permute-start.13 = (bf16[64,1024]{1,0:T(8,128)(2,1)}, bf16[64,1024]{1,0:T(8,128)(2,1)S(1)}, u32[]{:S(2)}, u32[]{:S(2)}) collective-permute-start(bf16[64,1024]{1,0:T(8,128)(2,1)} %get-tuple-element.57), channel_id=1, source_target_pairs={{0,24},{4,28},{8,16},{12,20},{16,8},{20,12},{24,0},{28,4},{1,25},{... | collective-permute-start | bytes 393224 | tf_op jit(solution)/shard_map/ppermute | solution.py:22
  13.6 17.0 %collective-permute-start.15 = (bf16[64,1024]{1,0:T(8,128)(2,1)}, bf16[64,1024]{1,0:T(8,128)(2,1)S(1)}, u32[]{:S(2)}, u32[]{:S(2)}) collective-permute-start(bf16[64,1024]{1,0:T(8,128)(2,1)} %get-tuple-element.58), channel_id=1, source_target_pairs={{0,28},{4,24},{8,20},{12,16},{16,12},{20,8},{24,4},{28,0},{1,29},{... | collective-permute-start | bytes 393224 | tf_op jit(solution)/shard_map/ppermute | solution.py:22
  24.5 7.6 %collective-permute-start.10 = (bf16[64,1024]{1,0:T(8,128)(2,1)S(1)}, bf16[64,1024]{1,0:T(8,128)(2,1)S(1)}, u32[]{:S(2)}, u32[]{:S(2)}) collective-permute-start(bf16[64,1024]{1,0:T(8,128)(2,1)S(1)} %collective-permute-done.9.refs_0_), channel_id=1, source_target_pairs={{0,2},{1,3},{2,0},{3,1},{4,6},{5,7},{6,4},{7,5},{8,10},{9,11},{10,... | collective-permute-start | bytes 393224 | tf_op jit(solution)/shard_map/ppermute | solution.py:22
  30.6 7.3 %collective-permute-start.16 = (bf16[64,1024]{1,0:T(8,128)(2,1)S(1)}, bf16[64,1024]{1,0:T(8,128)(2,1)S(1)}, u32[]{:S(2)}, u32[]{:S(2)}) collective-permute-start(bf16[64,1024]{1,0:T(8,128)(2,1)S(1)} %collective-permute-done.15.refs_6_), channel_id=1, source_target_pairs={{0,2},{1,3},{2,0},{3,1},{4,6},{5,7},{6,4},{7,5},{8,10},{9,11},{10,... | collective-permute-start | bytes 393224 | tf_op jit(solution)/shard_map/ppermute | solution.py:22
  38.0 18.7 %collective-permute-start.18 = (bf16[256,1024]{1,0:T(8,128)(2,1)S(1)}, bf16[256,1024]{1,0:T(8,128)(2,1)S(1)}, u32[]{:S(2)}, u32[]{:S(2)}) collective-permute-start(bf16[256,1024]{1,0:T(8,128)(2,1)S(1)} %get-tuple-element.60.refs_5_), channel_id=1, source_target_pairs={{0,1},{1,0},{2,3},{3,2},{4,5},{5,4},{6,7},{7,6},{8,9},{9,8},{10,11... | collective-permute-start | bytes 1572872 | tf_op jit(solution)/shard_map/ppermute | solution.py:22
  39.8 6.6 %collective-permute-start.3 = (bf16[64,1024]{1,0:T(8,128)(2,1)}, bf16[64,1024]{1,0:T(8,128)(2,1)S(1)}, u32[]{:S(2)}, u32[]{:S(2)}) collective-permute-start(bf16[64,1024]{1,0:T(8,128)(2,1)} %get-tuple-element.47), channel_id=1, source_target_pairs={{0,8},{4,12},{8,0},{12,4},{16,24},{20,28},{24,16},{28,20},{1,9},{5... | collective-permute-start | bytes 393224 | tf_op jit(solution)/shard_map/ppermute | solution.py:22
  40.5 7.7 %collective-permute-start.5 = (bf16[64,1024]{1,0:T(8,128)(2,1)}, bf16[64,1024]{1,0:T(8,128)(2,1)S(1)}, u32[]{:S(2)}, u32[]{:S(2)}) collective-permute-start(bf16[64,1024]{1,0:T(8,128)(2,1)} %get-tuple-element.48), channel_id=1, source_target_pairs={{0,12},{4,8},{8,4},{12,0},{16,28},{20,24},{24,20},{28,16},{1,13},{... | collective-permute-start | bytes 393224 | tf_op jit(solution)/shard_map/ppermute | solution.py:22
  41.6 13.7 %collective-permute-start = (bf16[64,1024]{1,0:T(8,128)(2,1)}, bf16[64,1024]{1,0:T(8,128)(2,1)S(1)}, u32[]{:S(2)}, u32[]{:S(2)}) collective-permute-start(bf16[64,1024]{1,0:T(8,128)(2,1)} %get-tuple-element.45.refs_0_), channel_id=1, source_target_pairs={{0,2},{1,3},{2,0},{3,1},{4,6},{5,7},{6,4},{7,5},{8,10},{9,11},{10,... | collective-permute-start | bytes 393224 | tf_op jit(solution)/shard_map/ppermute | solution.py:22
  44.2 11.8 %collective-permute-start.2 = (bf16[64,1024]{1,0:T(8,128)(2,1)S(1)}, bf16[64,1024]{1,0:T(8,128)(2,1)S(1)}, u32[]{:S(2)}, u32[]{:S(2)}) collective-permute-start(bf16[64,1024]{1,0:T(8,128)(2,1)S(1)} %collective-permute-done.1.refs_2_), channel_id=1, source_target_pairs={{0,2},{1,3},{2,0},{3,1},{4,6},{5,7},{6,4},{7,5},{8,10},{9,11},{10,... | collective-permute-start | bytes 393224 | tf_op jit(solution)/shard_map/ppermute | solution.py:22
  46.4 9.5 %collective-permute-start.4 = (bf16[64,1024]{1,0:T(8,128)(2,1)S(1)}, bf16[64,1024]{1,0:T(8,128)(2,1)S(1)}, u32[]{:S(2)}, u32[]{:S(2)}) collective-permute-start(bf16[64,1024]{1,0:T(8,128)(2,1)S(1)} %collective-permute-done.3.refs_4_), channel_id=1, source_target_pairs={{0,2},{1,3},{2,0},{3,1},{4,6},{5,7},{6,4},{7,5},{8,10},{9,11},{10,... | collective-permute-start | bytes 393224 | tf_op jit(solution)/shard_map/ppermute | solution.py:22
  48.2 7.8 %collective-permute-start.6 = (bf16[64,1024]{1,0:T(8,128)(2,1)S(1)}, bf16[64,1024]{1,0:T(8,128)(2,1)S(1)}, u32[]{:S(2)}, u32[]{:S(2)}) collective-permute-start(bf16[64,1024]{1,0:T(8,128)(2,1)S(1)} %collective-permute-done.5.refs_6_), channel_id=1, source_target_pairs={{0,2},{1,3},{2,0},{3,1},{4,6},{5,7},{6,4},{7,5},{8,10},{9,11},{10,... | collective-permute-start | bytes 393224 | tf_op jit(solution)/shard_map/ppermute | solution.py:22
  55.3 48.5 %collective-permute-start.32 = (bf16[1,208,384]{2,1,0:T(8,128)(2,1)S(1)}, bf16[1,208,384]{2,1,0:T(8,128)(2,1)S(1)}, u32[]{:S(2)}, u32[]{:S(2)}) collective-permute-start(bf16[1,208,384]{2,1,0:T(8,128)(2,1)S(1)} %copy-done.40), channel_id=1, source_target_pairs={{0,8},{4,12},{8,0},{12,4},{16,24},{20,28},{24,16},{28,20},{1,9},{5... | collective-permute-start | bytes 479240 | tf_op jit(solution)/shard_map/ppermute | solution.py:22
  56.1 8.6 %collective-permute-start.8 = (bf16[256,1024]{1,0:T(8,128)(2,1)S(1)}, bf16[256,1024]{1,0:T(8,128)(2,1)S(1)}, u32[]{:S(2)}, u32[]{:S(2)}) collective-permute-start(bf16[256,1024]{1,0:T(8,128)(2,1)S(1)} %get-tuple-element.52.refs_4_), channel_id=1, source_target_pairs={{0,1},{1,0},{2,3},{3,2},{4,5},{5,4},{6,7},{7,6},{8,9},{9,8},{10,11... | collective-permute-start | bytes 1572872 | tf_op jit(solution)/shard_map/ppermute | solution.py:22
  56.6 9.5 %collective-permute-start.7 = (bf16[256,1024]{1,0:T(8,128)(2,1)S(1)}, bf16[256,1024]{1,0:T(8,128)(2,1)S(1)}, u32[]{:S(2)}, u32[]{:S(2)}) collective-permute-start(bf16[256,1024]{1,0:T(8,128)(2,1)S(1)} %get-tuple-element.49.refs_2_), channel_id=1, source_target_pairs={{0,1},{1,0},{2,3},{3,2},{4,5},{5,4},{6,7},{7,6},{8,9},{9,8},{10,11... | collective-permute-start | bytes 1572872 | tf_op jit(solution)/shard_map/ppermute | solution.py:22
  64.1 8.1 %collective-permute-start.24 = (bf16[256,1024]{1,0:T(8,128)(2,1)S(1)}, bf16[256,1024]{1,0:T(8,128)(2,1)S(1)}, u32[]{:S(2)}, u32[]{:S(2)}) collective-permute-start(bf16[256,1024]{1,0:T(8,128)(2,1)S(1)} %convolution_convert_fusion), channel_id=1, source_target_pairs={{0,1},{1,0},{2,3},{3,2},{4,5},{5,4},{6,7},{7,6},{8,9},{9,8},{10,11... | collective-permute-start | bytes 1572872 | tf_op jit(solution)/shard_map/ppermute | solution.py:22
  71.4 9.2 %collective-permute-start.20 = (bf16[256,512]{1,0:T(8,128)(2,1)S(1)}, bf16[256,512]{1,0:T(8,128)(2,1)S(1)}, u32[]{:S(2)}, u32[]{:S(2)}) collective-permute-start(bf16[256,512]{1,0:T(8,128)(2,1)S(1)} %add_convert_fusion.3), channel_id=1, source_target_pairs={{0,2},{1,3},{2,0},{3,1},{4,6},{5,7},{6,4},{7,5},{8,10},{9,11},{10,... | collective-permute-start | bytes 786440 | tf_op jit(solution)/shard_map/ppermute | solution.py:22
  72.7 12.7 %collective-permute-start.25 = (bf16[256,512]{1,0:T(8,128)(2,1)S(1)}, bf16[256,512]{1,0:T(8,128)(2,1)S(1)}, u32[]{:S(2)}, u32[]{:S(2)}) collective-permute-start(bf16[256,512]{1,0:T(8,128)(2,1)S(1)} %add_convert_fusion.1), channel_id=1, source_target_pairs={{0,2},{1,3},{2,0},{3,1},{4,6},{5,7},{6,4},{7,5},{8,10},{9,11},{10,... | collective-permute-start | bytes 786440 | tf_op jit(solution)/shard_map/ppermute | solution.py:22
  80.8 10.6 %collective-permute-start.21 = (bf16[64,512]{1,0:T(8,128)(2,1)S(1)}, bf16[64,512]{1,0:T(8,128)(2,1)S(1)}, u32[]{:S(2)}, u32[]{:S(2)}) collective-permute-start(bf16[64,512]{1,0:T(8,128)(2,1)S(1)} %get-tuple-element.95), channel_id=1, source_target_pairs={{0,4},{4,0},{8,12},{12,8},{16,20},{20,16},{24,28},{28,24},{1,5},{5... | collective-permute-start | bytes 196616 | tf_op jit(solution)/shard_map/ppermute | solution.py:22
  85.6 12.1 %collective-permute-start.26 = (bf16[64,512]{1,0:T(8,128)(2,1)S(1)}, bf16[64,512]{1,0:T(8,128)(2,1)S(1)}, u32[]{:S(2)}, u32[]{:S(2)}) collective-permute-start(bf16[64,512]{1,0:T(8,128)(2,1)S(1)} %get-tuple-element.92), channel_id=1, source_target_pairs={{0,16},{4,20},{8,24},{12,28},{16,0},{20,4},{24,8},{28,12},{1,17},{... | collective-permute-start | bytes 196616 | tf_op jit(solution)/shard_map/ppermute | solution.py:22
  91.4 9.3 %collective-permute-start.27 = (bf16[64,512]{1,0:T(8,128)(2,1)S(1)}, bf16[64,512]{1,0:T(8,128)(2,1)S(1)}, u32[]{:S(2)}, u32[]{:S(2)}) collective-permute-start(bf16[64,512]{1,0:T(8,128)(2,1)S(1)} %get-tuple-element.91), channel_id=1, source_target_pairs={{0,20},{4,16},{8,28},{12,24},{16,4},{20,0},{24,12},{28,8},{1,21},{... | collective-permute-start | bytes 196616 | tf_op jit(solution)/shard_map/ppermute | solution.py:22
  93.7 7.0 %collective-permute-start.28 = (bf16[64,512]{1,0:T(8,128)(2,1)S(1)}, bf16[64,512]{1,0:T(8,128)(2,1)S(1)}, u32[]{:S(2)}, u32[]{:S(2)}) collective-permute-start(bf16[64,512]{1,0:T(8,128)(2,1)S(1)} %get-tuple-element.90), channel_id=1, source_target_pairs={{0,24},{4,28},{8,16},{12,20},{16,8},{20,12},{24,0},{28,4},{1,25},{... | collective-permute-start | bytes 196616 | tf_op jit(solution)/shard_map/ppermute | solution.py:22
  95.7 7.1 %collective-permute-start.29 = (bf16[64,512]{1,0:T(8,128)(2,1)S(1)}, bf16[64,512]{1,0:T(8,128)(2,1)S(1)}, u32[]{:S(2)}, u32[]{:S(2)}) collective-permute-start(bf16[64,512]{1,0:T(8,128)(2,1)S(1)} %get-tuple-element.89), channel_id=1, source_target_pairs={{0,28},{4,24},{8,20},{12,16},{16,12},{20,8},{24,4},{28,0},{1,29},{... | collective-permute-start | bytes 196616 | tf_op jit(solution)/shard_map/ppermute | solution.py:22
  103.9 14.4 %collective-permute-start.33 = (bf16[2,208,384]{2,1,0:T(8,128)(2,1)S(1)}, bf16[2,208,384]{2,1,0:T(8,128)(2,1)S(1)}, u32[]{:S(2)}, u32[]{:S(2)}) collective-permute-start(bf16[2,208,384]{2,1,0:T(8,128)(2,1)S(1)} %pad_maximum_fusion.3), channel_id=1, source_target_pairs={{0,16},{4,20},{8,24},{12,28},{16,0},{20,4},{24,8},{28,12},{1,17},{... | collective-permute-start | bytes 958472 | tf_op jit(solution)/shard_map/ppermute | solution.py:22
  108.9 9.6 %collective-permute-start.31 = (bf16[192,1024]{1,0:T(8,128)(2,1)S(1)}, bf16[192,1024]{1,0:T(8,128)(2,1)S(1)}, u32[]{:S(2)}, u32[]{:S(2)}) collective-permute-start(bf16[192,1024]{1,0:T(8,128)(2,1)S(1)} %pad_maximum_fusion.2.mine_ref), channel_id=1, source_target_pairs={{0,1},{1,0},{2,3},{3,2},{4,5},{5,4},{6,7},{7,6},{8,9},{9,8},{10,11... | collective-permute-start | bytes 1179656 | tf_op jit(solution)/shard_map/ppermute | solution.py:22
  118.3 22.3 %collective-permute-start.34 = (bf16[4,208,384]{2,1,0:T(8,128)(2,1)S(1)}, bf16[4,208,384]{2,1,0:T(8,128)(2,1)S(1)}, u32[]{:S(2)}, u32[]{:S(2)}) collective-permute-start(bf16[4,208,384]{2,1,0:T(8,128)(2,1)S(1)} %constant_dynamic-update-slice_fusion.7.wide_ref), channel_id=1, source_target_pairs={{0,4},{4,0},{8,12},{12,8},{16,20},{20,16},{24,28},{28,24},{1,5},{5... | collective-permute-start | bytes 1916936 | tf_op jit(solution)/shard_map/ppermute | solution.py:22
  120.2 25.6 %all-to-all-start = ((bf16[8,96,256]{2,1,0:T(8,128)(2,1)}), bf16[8,96,256]{2,1,0:T(8,128)(2,1)}, u32[]{:S(2)}, u32[]{:S(2)}) async-start(bf16[8,96,256]{2,1,0:T(8,128)(2,1)} %copy-done.4), calls=%async_computation | async-start | bytes 786432 | tf_op jit(solution)/shard_map/all_to_all | solution.py:553
  141.4 10.6 %collective-permute-start.37 = (bf16[48,384]{1,0:T(8,128)(2,1)S(1)}, bf16[48,384]{1,0:T(8,128)(2,1)S(1)}, u32[]{:S(2)}, u32[]{:S(2)}) collective-permute-start(bf16[48,384]{1,0:T(8,128)(2,1)S(1)} %shard_map.206), channel_id=1, source_target_pairs={{0,8},{4,12},{8,0},{12,4},{16,24},{20,28},{24,16},{28,20},{1,9},{5... | collective-permute-start | bytes 110600 | tf_op jit(solution)/shard_map/ppermute | solution.py:22
  142.9 9.1 %collective-permute-start.38 = (bf16[48,384]{1,0:T(8,128)(2,1)S(1)}, bf16[48,384]{1,0:T(8,128)(2,1)S(1)}, u32[]{:S(2)}, u32[]{:S(2)}) collective-permute-start(bf16[48,384]{1,0:T(8,128)(2,1)S(1)} %shard_map.206), channel_id=1, source_target_pairs={{0,16},{4,20},{8,24},{12,28},{16,0},{20,4},{24,8},{28,12},{1,17},{... | collective-permute-start | bytes 110600 | tf_op jit(solution)/shard_map/ppermute | solution.py:22
  145.2 6.7 %collective-permute-start.39 = (bf16[48,384]{1,0:T(8,128)(2,1)S(1)}, bf16[48,384]{1,0:T(8,128)(2,1)S(1)}, u32[]{:S(2)}, u32[]{:S(2)}) collective-permute-start(bf16[48,384]{1,0:T(8,128)(2,1)S(1)} %shard_map.206), channel_id=1, source_target_pairs={{0,24},{4,28},{8,16},{12,20},{16,8},{20,12},{24,0},{28,4},{1,25},{... | collective-permute-start | bytes 110600 | tf_op jit(solution)/shard_map/ppermute | solution.py:22
  145.8 7.2 %collective-permute-start.35 = (bf16[8,96,256]{2,1,0:T(8,128)(2,1)}, bf16[8,96,256]{2,1,0:T(8,128)(2,1)S(1)}, u32[]{:S(2)}, u32[]{:S(2)}) collective-permute-start(bf16[8,96,256]{2,1,0:T(8,128)(2,1)} %all-to-all-done), channel_id=1, source_target_pairs={{0,1},{1,0},{2,3},{3,2},{4,5},{5,4},{6,7},{7,6},{8,9},{9,8},{10,11... | collective-permute-start | bytes 1179656 | tf_op jit(solution)/shard_map/ppermute | solution.py:22
  (51 other events, 279.0 us)

commit v2 on v1

--- a/solution.py
+++ b/solution.py
@@ -14,7 +14,8 @@
 ALONG = (((0,), (0,)), ((), ()))
 CHUNKS = 2
 START_VMEM = 60 << 20
-WEIGHTS_VMEM = 52 << 20
+WEIGHTS_VMEM = 46 << 20
+INNER_MB = 58
 
 
 def swap(x, axis, offset):
@@ -56,7 +57,7 @@
 
 
 def start_kernel(tp_ref, sp_ref, *refs, slots, blocks, heads, key_dim, value_dim):
-    sources, outs, scratch, arrivals = refs[:9], refs[9 : 17 + blocks], refs[17 + blocks : -1], refs[-1]
+    sources, outs, scratch, arrivals = refs[:8], refs[8 : 14 + blocks], refs[14 + blocks : -1], refs[-1]
     send_refs, outs = outs[:blocks], outs[blocks:]
     columns = scratch[3].shape[1]
     start = pl.multiple_of(tp_ref[0] * columns, 128)
@@ -124,24 +125,16 @@
     return high, middle, (rest - middle.astype(F32)).astype(BF16)
 
 
-def prepare_part(log_ref, q_ref, k_ref, state_ref, kept_ref, decay_ref, decay_t_ref, scores_t_ref, qe_ref, sum_ref, incoming_ref, wide_ref, *, heads, key_dim, value_dim):
+def prepare_part(log_ref, q_ref, state_ref, kept_ref, qe_ref, sum_ref, flat_ref, incoming_ref, wide_ref, *, heads, key_dim, value_dim):
     tokens = q_ref.shape[0]
     row = lax.broadcasted_iota(jnp.int32, (tokens, tokens), 0)
     col = lax.broadcasted_iota(jnp.int32, (tokens, tokens), 1)
     below = jnp.where(col <= row, 1.0, 0.0).astype(BF16)
     terms = three_terms(log_ref[...])
     sums = sum([dot(below, term, ACROSS) for term in terms])
-    flats = sum([dot(term, below, ACROSS) for term in terms])
     sum_ref[...] = sums[:, :heads]
-    q, k = q_ref[...], k_ref[...]
-    for head in range(heads):
-        down = sums[:, head : head + 1]
-        flat = flats[head : head + 1, :]
-        decay = jnp.where(row >= col, jnp.exp(jnp.minimum(down - flat, 0.0)), 0.0)
-        decay_t = jnp.where(col >= row, jnp.exp(jnp.minimum(flat - down, 0.0)), 0.0)
-        decay_ref[head] = decay
-        decay_t_ref[head] = decay_t
-        scores_t_ref[head] = (dot(masked(k, head, key_dim), q, ACROSS) * decay_t).astype(BF16)
+    flat_ref[...] = sum([dot(term, below, ACROSS) for term in terms])[:heads]
+    q = q_ref[...]
     qe_ref[...] = (q.astype(F32) * spread_heads(jnp.exp(sums), q.shape, key_dim)).astype(BF16)
     width = heads * value_dim
     from_lane = lax.broadcasted_iota(jnp.int32, (value_dim, width), 0)
@@ -164,12 +157,12 @@
         wide_ref[block, tokens:, :] = extra
 
 
-def order_kernel(tp_ref, sp_ref, wide_ref, last_ref, own_ref, other_ref, sums_ref, *, turn):
+def order_kernel(tp_ref, sp_ref, wide_ref, last_ref, own_ref, other_ref, sums_ref):
     kept, rows, _ = wide_ref.shape
     half = (rows - 16) // 2
     own = pl.multiple_of((tp_ref[0] & 1) * half, 16)
     for position in range(2 * kept):
-        offset = sum(bit for step, bit in enumerate(turn) if position >> step & 1)
+        offset = 2 * position if position < kept else 2 * (position - kept) + 1
         ref, at = (wide_ref, position) if position < kept else (last_ref, position - kept)
         block = sp_ref[0] ^ offset
         target = pl.ds(pl.multiple_of(block * half, 16), half)
@@ -187,29 +180,27 @@
     pair_ref[...] = (first + decay * second).astype(BF16)
 
 
-def inject_kernel(stream_ref, proj_ref, qe_ref, o_ref, inject_ref, *, heads, key_dim, value_dim):
-    o = dot(stream_ref[...], proj_ref[...], ACROSS).astype(BF16)
-    o_ref[...] = o
-    cross = dot(qe_ref[...], o, ALONG)
-    packed = jnp.zeros((key_dim, heads * value_dim), F32)
-    for head in range(heads):
-        packed = packed + masked(cross[head * key_dim : (head + 1) * key_dim], head, value_dim)
-    inject_ref[...] = packed.astype(BF16)
-
-
-def inner_kernel(o_ref, v_ref, q_ref, k_ref, decay_ref, decay_t_ref, scores_t_ref, sum_ref, state_ref, query_ref, key_ref, value_ref, *, heads, key_dim, value_dim):
+def inner_kernel(o_ref, v_ref, q_ref, k_ref, sum_ref, flat_ref, state_ref, query_ref, key_ref, value_ref, *, heads, key_dim, value_dim):
     o, v, q, k = o_ref[...], v_ref[...], q_ref[...], k_ref[...]
-    growth = spread_heads(jnp.exp(sum_ref[...]), q.shape, key_dim)
-    query = growth * dot(o, state_ref[...], ACROSS)
+    tokens = q.shape[0]
+    row = lax.broadcasted_iota(jnp.int32, (tokens, tokens), 0)
+    col = lax.broadcasted_iota(jnp.int32, (tokens, tokens), 1)
+    sums = sum_ref[...]
+    query = spread_heads(jnp.exp(sums), q.shape, key_dim) * dot(o, state_ref[...], ACROSS)
     key = jnp.zeros(k.shape, F32)
     value = jnp.zeros(v.shape, F32)
     for head in range(heads):
+        down, flat = sums[:, head : head + 1], flat_ref[head : head + 1, :]
+        decay = jnp.where(row >= col, jnp.exp(jnp.minimum(down - flat, 0.0)), 0.0)
+        decay_t = jnp.where(col >= row, jnp.exp(jnp.minimum(flat - down, 0.0)), 0.0)
         o_head = masked(o, head, value_dim)
-        prob = (dot(o_head, v, ACROSS) * decay_ref[head]).astype(BF16)
-        prob_t = (dot(v, o_head, ACROSS) * decay_t_ref[head]).astype(BF16)
-        query = query + dot(prob, masked(k, head, key_dim))
+        k_head = masked(k, head, key_dim)
+        prob = (dot(o_head, v, ACROSS) * decay).astype(BF16)
+        prob_t = (dot(v, o_head, ACROSS) * decay_t).astype(BF16)
+        scores_t = (dot(k_head, q, ACROSS) * decay_t).astype(BF16)
+        query = query + dot(prob, k_head)
         key = key + dot(prob_t, masked(q, head, key_dim))
-        value = value + dot(scores_t_ref[head], o_head)
+        value = value + dot(scores_t, o_head)
     query_ref[...] = query.astype(BF16)
     key_ref[...] = key
     value_ref[...] = value
@@ -273,7 +264,23 @@
         out[...] = sum([dot(p, g[...], ALONG) for p, g in zip(pieces, grads)]).astype(BF16)
 
 
-def stream_kernel(at_ref, mine_ref, other_ref, stream_ref, send_ref, *, even, columns):
+def combine_kernel(pick_ref, grad_ref, *refs):
+    *pieces, stream_ref, joined = refs
+    slots = pieces[0].shape[0]
+    for k, piece in enumerate(pieces):
+        joined[k * slots : (k + 1) * slots, :] = piece[...]
+    total = grad_ref[...].astype(F32) + dot(pick_ref[...], joined[...])
+    stream_ref[...] = total.astype(BF16)
+
+
+def project_kernel(columns_ref, rows_ref, *refs):
+    total = dot(columns_ref[...], rows_ref[...], ALONG)
+    if len(refs) == 2:
+        total = total + refs[0][...]
+    refs[-1][...] = total
+
+
+def stream_kernel(at_ref, mine_ref, other_ref, proj_ref, qe_ref, send_ref, o_ref, inject_ref, stream_ref, *, even, columns, heads, key_dim, value_dim):
     _, half, out_columns = send_ref.shape
     per_piece = columns // out_columns
     row = pl.multiple_of((at_ref[0] & 1) * half, 16)
@@ -286,6 +293,13 @@
                 send_ref[place * per_piece + b] = ref[
                     pl.ds(row, half), pl.ds(position * columns + b * out_columns, out_columns)
                 ]
+    o = dot(stream_ref[...], proj_ref[...], ACROSS).astype(BF16)
+    o_ref[...] = o
+    cross = dot(qe_ref[...], o, ALONG)
+    packed = jnp.zeros((key_dim, heads * value_dim), F32)
+    for head in range(heads):
+        packed = packed + masked(cross[head * key_dim : (head + 1) * key_dim], head, value_dim)
+    inject_ref[...] = packed.astype(BF16)
 
 
 def assemble_kernel(*refs):
@@ -304,15 +318,20 @@
     return jax.ShapeDtypeStruct(shape, dtype)
 
 
-def call(kernel, out_shape, flops, *args, megabytes=12, **settings):
+def call(kernel, out_shape, flops, *args, megabytes=12, scratch=(), plain=False, plain_outs=(), **settings):
+    space = None if plain else pltpu.VMEM
+    out_space = pltpu.VMEM
+    shapes, tree = jax.tree.flatten(out_shape)
+    outs = [pl.BlockSpec(memory_space=None if n in plain_outs else out_space) for n in range(len(shapes))]
     return pl.pallas_call(
         functools.partial(kernel, **settings) if settings else kernel,
         in_specs=[
-            pl.BlockSpec(memory_space=pltpu.SMEM if arg.dtype == jnp.int32 and arg.ndim == 1 else pltpu.VMEM)
+            pl.BlockSpec(memory_space=pltpu.SMEM if arg.dtype == jnp.int32 and arg.ndim == 1 else space)
             for arg in args
         ],
-        out_specs=jax.tree.map(lambda _: pl.BlockSpec(memory_space=pltpu.VMEM), out_shape),
+        out_specs=jax.tree.unflatten(tree, outs),
         out_shape=out_shape,
+        scratch_shapes=scratch,
         compiler_params=pltpu.CompilerParams(vmem_limit_bytes=megabytes << 20),
         cost_estimate=pl.CostEstimate(flops=flops, bytes_accessed=1 << 20, transcendentals=0),
     )(*args)
@@ -360,7 +379,6 @@
     log_rows = log_decay.T
     if heads == 1:
         log_rows = jnp.pad(log_rows, ((0, 7), (0, 0)))
-    square = (heads, tokens_here, tokens_here)
     sources = (
         expert_ids.T,
         expert_weights.T,
@@ -368,7 +386,6 @@
         out_grad,
         log_rows,
         queries,
-        keys,
         incoming_state[0],
         retained,
     )
@@ -379,11 +396,9 @@
     (
         *to_send,
         picker,
-        decay,
-        decay_t,
-        scores_t,
         grown,
         running_total,
+        flat_total,
         incoming,
         wide,
     ) = pl.pallas_call(
@@ -391,15 +406,13 @@
             start_kernel, slots=slots, blocks=sp_count, heads=heads, key_dim=key_dim, value_dim=value_dim
         ),
         in_specs=[smem, smem] + [hbm] * len(sources),
-        out_specs=[vmem] * sp_count + [plain] * 8,
+        out_specs=[vmem] * sp_count + [plain] * 6,
         out_shape=[shaped((slots, 2 * columns), BF16)] * sp_count
         + [
             shaped((tokens_here, slot_count), BF16),
-            shaped(square, F32),
-            shaped(square, F32),
-            shaped(square, BF16),
             shaped(queries.shape, BF16),
             shaped(log_decay.shape, F32),
+            shaped(log_decay.shape[::-1], F32),
             shaped((key_width, value_width), BF16),
             shaped((1, tokens_here + 16, value_width), BF16),
         ],
@@ -518,58 +531,58 @@
         *rows_other,
     )
 
-    token_grad = dot(picker, jnp.concatenate(returned, axis=0))
-    stream_part = (out_grad.astype(F32) + token_grad).astype(BF16)
+    stream_part = call(
+        combine_kernel, shaped(out_grad.shape, BF16), 1 << 27, picker, out_grad, *returned,
+        scratch=[pltpu.VMEM((slot_count, columns), BF16)],
+    )
     stream_mine = jnp.concatenate(far_pieces(stream_part), axis=1)
     stream_other = near(stream_mine)
     half = tokens_here // 2
     out_columns = width // sp_count
-    stream, columns_out = call(
+    sizes = dict(heads=heads, key_dim=key_dim, value_dim=value_dim)
+    columns_out, o, added = call(
         functools.partial(stream_kernel, even=even, columns=columns),
-        [shaped((tokens_here, width), BF16), shaped((sp_count, half, out_columns), BF16)],
+        [
+            shaped((sp_count, half, out_columns), BF16),
+            shaped((tokens_here, value_width), BF16),
+            shaped((key_dim, value_width), BF16),
+        ],
         1 << 28,
         tp_at.reshape(1),
         stream_mine,
         stream_other,
-    )
-
-    sp_bits = powers(sp_count)
-    turn = sp_bits[1:] + sp_bits[:1]
-    for bit in turn[:-1]:
-        wide = jnp.concatenate([wide, swap(wide, "sp", bit)], axis=0)
-    last = swap(wide, "sp", turn[-1])
+        out_proj,
+        grown,
+        scratch=[pltpu.VMEM((tokens_here, width), BF16)],
+        plain_outs=(1, 2),
+        **sizes,
+    )
+
+    kept = [wide]
+    for k in range(2, sp_count, 2):
+        kept.append(swap(wide, "sp", k))
+    near_kept = jnp.concatenate(kept, axis=0)
+    far_kept = swap(near_kept, "sp", 1)
 
     halves = shaped((sp_count * half, value_width), BF16)
     own_rows, other_rows, block_sums = call(
-        functools.partial(order_kernel, turn=tuple(turn)),
+        order_kernel,
         [halves, halves, shaped((sp_count, value_width), F32)],
         1 << 28,
         tp_at.reshape(1),
         sp_at.reshape(1),
-        wide,
-        last,
+        near_kept,
+        far_kept,
     )
 
     got_half = lax.all_to_all(columns_out, "sp", split_axis=0, concat_axis=0, tiled=True)
     other_half = near(got_half)
     own_cols = got_half.reshape(-1, out_columns)
     other_cols = other_half.reshape(-1, out_columns)
-    own_part = dot(own_cols, own_rows, ALONG)
-    out_proj_grad = own_part + dot(other_cols, other_rows, ALONG)
-
-    sizes = dict(heads=heads, key_dim=key_dim, value_dim=value_dim)
-    o, added = call(
-        inject_kernel,
-        [
-            shaped((tokens_here, value_width), BF16),
-            shaped((key_dim, value_width), BF16),
-        ],
-        1 << 30,
-        stream,
-        out_proj,
-        grown,
-        **sizes,
-    )
+    product = shaped((out_columns, value_width), F32)
+    own_part = call(project_kernel, product, 1 << 28, own_cols, own_rows)
+    out_proj_grad = call(project_kernel, product, 1 << 28, other_cols, other_rows, own_part)
+
     partner = swap(added, "sp", 1)
     pair = call(pair_kernel, shaped(added.shape, BF16), 1 << 26, sp_at.reshape(1), block_sums, added, partner)
     arrived = [partner]
@@ -584,11 +597,11 @@
         values,
         queries,
         keys,
-        decay,
-        decay_t,
-        scores_t,
         running_total,
+        flat_total,
         incoming,
+        megabytes=INNER_MB,
+        plain=True,
         **sizes,
     )
 

time: 156 us -> 145 us (0.929)
  local copies, waits for them, and re-layouts: 12.7 us -> 7.39 us
  waiting for transfers between devices: 51.6 us -> 46.7 us
  matrix products: 14.8 us -> 9.96 us
  starting transfers between devices: 52.8 us -> 56.9 us
    unnamed x92 -> x65, local copies, waits for them, and re-layouts: 12.6 us -> 7.33 us
    ppermute x40 -> x41, waiting for transfers between devices: 51.6 us -> 46.7 us  [swap(): return lax.ppermute(x, axis, [(d, d ^ offset) for d in range(count)])]
    dot_general x17 -> x14, matrix products: 14.8 us -> 9.96 us  [dot(): return lax.dot_general(a, b, dims, preferred_element_type=F32)]
    ppermute x40 -> x41, starting transfers between devices: 48.4 us -> 52.9 us  [swap(): return lax.ppermute(x, axis, [(d, d ^ offset) for d in range(count)])]
    pallas_call x8 -> x10, Pallas kernels: 4.25 us -> 7.72 us  [call(): pl.pallas_call(functools.partial(kernel, **settings) if settings else ker...]
    pallas_call x1, Pallas kernels: 5.28 us -> 2.92 us  [on_device(): pl.pallas_call(functools.partial(weights_kernel, even=even, columns=colum...]
  transfers between devices with their start and end apart: 41 -> 42, of which waited for: 17 -> 17; matrix products, arithmetic and copies ran while one was open for 8% -> 7% of each run, Pallas kernels for 11% -> 12%
where the time goes in v2:
time: 145 us
  starting transfers between devices  56.9 us (39%)
  waiting for transfers between devices  46.7 us (32%)
  Pallas kernels  22.2 us (15%)
  matrix products  9.96 us (7%)
  local copies, waits for them, and re-layouts  7.39 us (5%)
    ppermute x41, starting transfers between devices, swap(): return lax.ppermute(x, axis, [(d, d ^ offset) for d in range(count)])  52.9 us
    ppermute x41, waiting for transfers between devices, swap(): return lax.ppermute(x, axis, [(d, d ^ offset) for d in range(count)])  46.7 us
    dot_general x14, matrix products, dot(): return lax.dot_general(a, b, dims, preferred_element_type=F32)  9.96 us
    pallas_call x2, Pallas kernels, gradients(): pl.pallas_call(kernel, grid_spec=pltpu.PrefetchScalarGridSpec(num_scalar_...  8.53 us
    pallas_call x10, Pallas kernels, call(): pl.pallas_call(functools.partial(kernel, **settings) if settings else ker...  7.72 us
    unnamed x65, local copies, waits for them, and re-layouts  7.33 us
    all_to_all x1, starting transfers between devices, on_device(): lax.all_to_all(columns_out, 'sp', split_axis=0, concat_axis=0, tiled=True)  3.99 us
    pallas_call x1, Pallas kernels, on_device(): pl.pallas_call(functools.partial(start_kernel, slots=slots, blocks=sp_cou...  3.08 us
  transfers between devices with their start and end apart: 42, of which 17 were waited for; matrix products, arithmetic and copies ran while one was open for 7% of the time, Pallas kernels for 12%

profile of v2, /device:TPU:0, one launch (start us, length us, event | category | flops | bytes accessed | tf_op | source)
XLA Modules:
  0.0 144.6 jit_solution(11475293284709217408)
XLA Ops:
  0.6 3.1 %start.1 = (bf16[64,1024]{1,0:T(8,128)(2,1)}, bf16[64,1024]{1,0:T(8,128)(2,1)}, bf16[64,1024]{1,0:T(8,128)(2,1)}, bf16[64,1024]{1,0:T(8,128)(2,1)}, bf16[64,1024...) custom-call(s32[1]{0:T(128)} %bitcast.tp_ref.at_ref, ...), custom_call_target="tpu_custom_call" | custom-call | flops 201326592 | bytes 1048576 | tf_op jit(solution)/shard_map/start/pallas_call | solution.py:404
  3.7 4.1 %collective-permute-start.9 = (bf16[64,1024]{1,0:T(8,128)(2,1)}, bf16[64,1024]{1,0:T(8,128)(2,1)S(1)}, u32[]{:S(2)}, u32[]{:S(2)}) collective-permute-start(bf16[64,1024]{1,0:T(8,128)(2,1)} %get-tuple-element.52), channel_id=1, source_target_pairs={{0,16},{4,20},{8,24},{12,28},{16,0},{20,4},{24,8},{28,12},{1,17},{... | collective-permute-start | bytes 393224 | tf_op jit(solution)/shard_map/ppermute | solution.py:23
  9.1 3.6 %collective-permute-start.13 = (bf16[64,1024]{1,0:T(8,128)(2,1)}, bf16[64,1024]{1,0:T(8,128)(2,1)S(1)}, u32[]{:S(2)}, u32[]{:S(2)}) collective-permute-start(bf16[64,1024]{1,0:T(8,128)(2,1)} %get-tuple-element.54), channel_id=1, source_target_pairs={{0,24},{4,28},{8,16},{12,20},{16,8},{20,12},{24,0},{28,4},{1,25},{... | collective-permute-start | bytes 393224 | tf_op jit(solution)/shard_map/ppermute | solution.py:23
  12.7 10.9 %collective-permute-done.9.refs_0_ = bf16[64,1024]{1,0:T(8,128)(2,1)S(1)} collective-permute-done((bf16[64,1024]{1,0:T(8,128)(2,1)}, bf16[64,1024]{1,0:T(8,128)(2,1)S(1)}, u32[]{:S(2)}, u32[]{:S(2)}) %collective-permute-start.9) | collective-permute-done | bytes 131104 | tf_op jit(solution)/shard_map/ppermute | solution.py:23
  23.7 1.8 %collective-permute-start.10 = (bf16[64,1024]{1,0:T(8,128)(2,1)S(1)}, bf16[64,1024]{1,0:T(8,128)(2,1)S(1)}, u32[]{:S(2)}, u32[]{:S(2)}) collective-permute-start(bf16[64,1024]{1,0:T(8,128)(2,1)S(1)} %collective-permute-done.9.refs_0_), channel_id=1, source_target_pairs={{0,2},{1,3},{2,0},{3,1},{4,6},{5,7},{6,4},{7,5},{8,10},{9,11},{10,... | collective-permute-start | bytes 393224 | tf_op jit(solution)/shard_map/ppermute | solution.py:23
  25.5 2.2 %collective-permute-done.11.refs_2_ = bf16[64,1024]{1,0:T(8,128)(2,1)S(1)} collective-permute-done((bf16[64,1024]{1,0:T(8,128)(2,1)}, bf16[64,1024]{1,0:T(8,128)(2,1)S(1)}, u32[]{:S(2)}, u32[]{:S(2)}) %collective-permute-start.11) | collective-permute-done | bytes 131104 | tf_op jit(solution)/shard_map/ppermute | solution.py:23
  31.3 2.8 %collective-permute-done.12.refs_3_ = bf16[64,1024]{1,0:T(8,128)(2,1)S(1)} collective-permute-done((bf16[64,1024]{1,0:T(8,128)(2,1)S(1)}, bf16[64,1024]{1,0:T(8,128)(2,1)S(1)}, u32[]{:S(2)}, u32[]{:S(2)}) %collective-permute-start.12) | collective-permute-done | bytes 131104 | tf_op jit(solution)/shard_map/ppermute | solution.py:23
  34.1 1.6 %collective-permute-done.14.refs_5_ = bf16[64,1024]{1,0:T(8,128)(2,1)S(1)} collective-permute-done((bf16[64,1024]{1,0:T(8,128)(2,1)S(1)}, bf16[64,1024]{1,0:T(8,128)(2,1)S(1)}, u32[]{:S(2)}, u32[]{:S(2)}) %collective-permute-start.14) | collective-permute-done | bytes 131104 | tf_op jit(solution)/shard_map/ppermute | solution.py:23
  37.2 1.8 %collective-permute-start.1 = (bf16[64,1024]{1,0:T(8,128)(2,1)}, bf16[64,1024]{1,0:T(8,128)(2,1)S(1)}, u32[]{:S(2)}, u32[]{:S(2)}) collective-permute-start(bf16[64,1024]{1,0:T(8,128)(2,1)} %get-tuple-element.43), channel_id=1, source_target_pairs={{0,4},{4,0},{8,12},{12,8},{16,20},{20,16},{24,28},{28,24},{1,5},{5... | collective-permute-start | bytes 393224 | tf_op jit(solution)/shard_map/ppermute | solution.py:23
  40.8 1.8 %collective-permute-start = (bf16[64,1024]{1,0:T(8,128)(2,1)}, bf16[64,1024]{1,0:T(8,128)(2,1)S(1)}, u32[]{:S(2)}, u32[]{:S(2)}) collective-permute-start(bf16[64,1024]{1,0:T(8,128)(2,1)} %get-tuple-element.42.refs_0_), channel_id=1, source_target_pairs={{0,2},{1,3},{2,0},{3,1},{4,6},{5,7},{6,4},{7,5},{8,10},{9,11},{10,... | collective-permute-start | bytes 393224 | tf_op jit(solution)/shard_map/ppermute | solution.py:23
  43.3 1.8 %collective-permute-start.2 = (bf16[64,1024]{1,0:T(8,128)(2,1)S(1)}, bf16[64,1024]{1,0:T(8,128)(2,1)S(1)}, u32[]{:S(2)}, u32[]{:S(2)}) collective-permute-start(bf16[64,1024]{1,0:T(8,128)(2,1)S(1)} %collective-permute-done.1.refs_2_), channel_id=1, source_target_pairs={{0,2},{1,3},{2,0},{3,1},{4,6},{5,7},{6,4},{7,5},{8,10},{9,11},{10,... | collective-permute-start | bytes 393224 | tf_op jit(solution)/shard_map/ppermute | solution.py:23
  47.3 1.8 %collective-permute-start.6 = (bf16[64,1024]{1,0:T(8,128)(2,1)S(1)}, bf16[64,1024]{1,0:T(8,128)(2,1)S(1)}, u32[]{:S(2)}, u32[]{:S(2)}) collective-permute-start(bf16[64,1024]{1,0:T(8,128)(2,1)S(1)} %collective-permute-done.5.refs_6_), channel_id=1, source_target_pairs={{0,2},{1,3},{2,0},{3,1},{4,6},{5,7},{6,4},{7,5},{8,10},{9,11},{10,... | collective-permute-start | bytes 393224 | tf_op jit(solution)/shard_map/ppermute | solution.py:23
  49.1 2.9 %weights.1 = (bf16[1024,1024]{1,0:T(8,128)(2,1)S(1)}, bf16[1024,1024]{1,0:T(8,128)(2,1)S(1)}, bf16[512,1024]{1,0:T(8,128)(2,1)S(1)}, bf16[512,1024]{1,0:T(8,128)(2,1)S(1)}) custom-call(s32[1]{0:T(128)} %bitcast.tp_ref.at_ref, bf16[2048,512]{1,0:T(8,128)(2,1)} %bitcast.34, bf16[2048,512]{1,0:T(8,128)(2,1)} %bitcast.35, bf16[512,2048]{1,0:T(8,128)(2,1)} %bitcast.36), custom_call_target="tpu_custom_call" | custom-call | flops 1073741824 | bytes 1048576 | tf_op jit(solution)/shard_map/weights/pallas_call | solution.py:443
  52.5 2.0 %collective-permute-done.6.refs_7_ = bf16[64,1024]{1,0:T(8,128)(2,1)S(1)} collective-permute-done((bf16[64,1024]{1,0:T(8,128)(2,1)S(1)}, bf16[64,1024]{1,0:T(8,128)(2,1)S(1)}, u32[]{:S(2)}, u32[]{:S(2)}) %collective-permute-start.6) | collective-permute-done | bytes 131104 | tf_op jit(solution)/shard_map/ppermute | solution.py:23
  65.5 1.8 %collective-permute-start.25 = (bf16[256,512]{1,0:T(8,128)(2,1)S(1)}, bf16[256,512]{1,0:T(8,128)(2,1)S(1)}, u32[]{:S(2)}, u32[]{:S(2)}) collective-permute-start(bf16[256,512]{1,0:T(8,128)(2,1)S(1)} %add_convert_fusion.1), channel_id=1, source_target_pairs={{0,2},{1,3},{2,0},{3,1},{4,6},{5,7},{6,4},{7,5},{8,10},{9,11},{10,... | collective-permute-start | bytes 786440 | tf_op jit(solution)/shard_map/ppermute | solution.py:23
  68.1 6.6 %collective-permute-done.25 = bf16[256,512]{1,0:T(8,128)(2,1)S(1)} collective-permute-done((bf16[256,512]{1,0:T(8,128)(2,1)S(1)}, bf16[256,512]{1,0:T(8,128)(2,1)S(1)}, u32[]{:S(2)}, u32[]{:S(2)}) %collective-permute-start.25) | collective-permute-done | bytes 262176 | tf_op jit(solution)/shard_map/ppermute | solution.py:23
  74.9 3.1 %collective-permute-start.26 = (bf16[64,512]{1,0:T(8,128)(2,1)S(1)}, bf16[64,512]{1,0:T(8,128)(2,1)S(1)}, u32[]{:S(2)}, u32[]{:S(2)}) collective-permute-start(bf16[64,512]{1,0:T(8,128)(2,1)S(1)} %get-tuple-element.86), channel_id=1, source_target_pairs={{0,16},{4,20},{8,24},{12,28},{16,0},{20,4},{24,8},{28,12},{1,17},{... | collective-permute-start | bytes 196616 | tf_op jit(solution)/shard_map/ppermute | solution.py:23
  78.9 2.9 %collective-permute-start.28 = (bf16[64,512]{1,0:T(8,128)(2,1)S(1)}, bf16[64,512]{1,0:T(8,128)(2,1)S(1)}, u32[]{:S(2)}, u32[]{:S(2)}) collective-permute-start(bf16[64,512]{1,0:T(8,128)(2,1)S(1)} %get-tuple-element.84), channel_id=1, source_target_pairs={{0,24},{4,28},{8,16},{12,20},{16,8},{20,12},{24,0},{28,4},{1,25},{... | collective-permute-start | bytes 196616 | tf_op jit(solution)/shard_map/ppermute | solution.py:23
  84.6 2.8 %collective-permute-done.27.refs_5_ = bf16[64,512]{1,0:T(8,128)(2,1)S(1)} collective-permute-done((bf16[64,512]{1,0:T(8,128)(2,1)S(1)}, bf16[64,512]{1,0:T(8,128)(2,1)S(1)}, u32[]{:S(2)}, u32[]{:S(2)}) %collective-permute-start.27) | collective-permute-done | bytes 65568 | tf_op jit(solution)/shard_map/ppermute | solution.py:23
  87.5 2.1 %collective-permute-done.29.refs_7_ = bf16[64,512]{1,0:T(8,128)(2,1)S(1)} collective-permute-done((bf16[64,512]{1,0:T(8,128)(2,1)S(1)}, bf16[64,512]{1,0:T(8,128)(2,1)S(1)}, u32[]{:S(2)}, u32[]{:S(2)}) %collective-permute-start.29) | collective-permute-done | bytes 65568 | tf_op jit(solution)/shard_map/ppermute | solution.py:23
  89.6 3.5 %collective-permute-done.23.refs_3_ = bf16[64,512]{1,0:T(8,128)(2,1)S(1)} collective-permute-done((bf16[64,512]{1,0:T(8,128)(2,1)S(1)}, bf16[64,512]{1,0:T(8,128)(2,1)S(1)}, u32[]{:S(2)}, u32[]{:S(2)}) %collective-permute-start.23) | collective-permute-done | bytes 65568 | tf_op jit(solution)/shard_map/ppermute | solution.py:23
  94.8 5.0 %collective-permute-start.34 = (bf16[1,208,384]{2,1,0:T(8,128)(2,1)S(1)}, bf16[1,208,384]{2,1,0:T(8,128)(2,1)S(1)}, u32[]{:S(2)}, u32[]{:S(2)}) collective-permute-start(bf16[1,208,384]{2,1,0:T(8,128)(2,1)S(1)} %copy-done.30), channel_id=1, source_target_pairs={{0,16},{4,20},{8,24},{12,28},{16,0},{20,4},{24,8},{28,12},{1,17},{... | collective-permute-start | bytes 479240 | tf_op jit(solution)/shard_map/ppermute | solution.py:23
  100.0 2.6 %collective-permute-done.33 = bf16[1,208,384]{2,1,0:T(8,128)(2,1)S(1)} collective-permute-done((bf16[1,208,384]{2,1,0:T(8,128)(2,1)S(1)}, bf16[1,208,384]{2,1,0:T(8,128)(2,1)S(1)}, u32[]{:S(2)}, u32[]{:S(2)}) %collective-permute-start.33) | collective-permute-done | bytes 159776 | tf_op jit(solution)/shard_map/ppermute | solution.py:23
  102.6 4.5 %collective-permute-done.34 = bf16[1,208,384]{2,1,0:T(8,128)(2,1)S(1)} collective-permute-done((bf16[1,208,384]{2,1,0:T(8,128)(2,1)S(1)}, bf16[1,208,384]{2,1,0:T(8,128)(2,1)S(1)}, u32[]{:S(2)}, u32[]{:S(2)}) %collective-permute-start.34) | collective-permute-done | bytes 159776 | tf_op jit(solution)/shard_map/ppermute | solution.py:23
  107.2 2.0 %collective-permute-start.36 = (bf16[4,208,384]{2,1,0:T(8,128)(2,1)S(1)}, bf16[4,208,384]{2,1,0:T(8,128)(2,1)S(1)}, u32[]{:S(2)}, u32[]{:S(2)}) collective-permute-start(bf16[4,208,384]{2,1,0:T(8,128)(2,1)S(1)} %constant_dynamic-update-slice_fusion.wide_ref), channel_id=1, source_target_pairs={{0,4},{4,0},{8,12},{12,8},{16,20},{20,16},{24,28},{28,24},{1,5},{5... | collective-permute-start | bytes 1916936 | tf_op jit(solution)/shard_map/ppermute | solution.py:23
  111.8 4.0 %all-to-all-start = ((bf16[8,96,256]{2,1,0:T(8,128)(2,1)}), bf16[8,96,256]{2,1,0:T(8,128)(2,1)S(1)}, u32[]{:S(2)}, u32[]{:S(2)}) async-start(bf16[8,96,256]{2,1,0:T(8,128)(2,1)} %copy-done.8), calls=%async_computation | async-start | bytes 786432 | tf_op jit(solution)/shard_map/all_to_all | solution.py:578
  119.8 4.7 %shard_map.200 = (bf16[2048,512]{1,0:T(8,128)(2,1)}, bf16[2048,512]{1,0:T(8,128)(2,1)}) custom-call(s32[4]{0:T(128)S(1)} %iota_xor_fusion.at_ref, bf16[256,512]{1,0:T(8,128)(2,1)S(1)} %copy-done.25, bf16[256,512]{1,0:T(8,128)(2,1)S(1)} %copy-done.21, bf16[256,512]{1,0:T(8,128)(2,1)S(1)} %copy-done.23, bf16[256,512]{1,0:T(8,128)(2,1)S(1)} %get-tuple-element.77.refs_3_, ...), custom_call_target="tpu_custom_call" | custom-call | flops 4294967296 | bytes 1048576 | tf_op jit(solution)/shard_map/pallas_call | solution.py:504
  124.5 2.0 %collective-permute-start.37 = (bf16[48,384]{1,0:T(8,128)(2,1)S(1)}, bf16[48,384]{1,0:T(8,128)(2,1)S(1)}, u32[]{:S(2)}, u32[]{:S(2)}) collective-permute-start(bf16[48,384]{1,0:T(8,128)(2,1)S(1)} %get-tuple-element.74.added_ref), channel_id=1, source_target_pairs={{0,4},{4,0},{8,12},{12,8},{16,20},{20,16},{24,28},{28,24},{1,5},{5... | collective-permute-start | bytes 110600 | tf_op jit(solution)/shard_map/ppermute | solution.py:23
  126.5 3.8 %shard_map.201 = bf16[512,2048]{1,0:T(8,128)(2,1)} custom-call(s32[4]{0:T(128)S(1)} %iota_xor_fusion.at_ref, bf16[256,512]{1,0:T(8,128)(2,1)S(1)} %copy-done.27, bf16[256,512]{1,0:T(8,128)(2,1)S(1)} %copy-done.26, bf16[256,1024]{1,0:T(8,128)(2,1)S(1)} %copy-done.15, bf16[256,1024]{1,0:T(8,128)(2,1)S(1)} %copy-done.13, bf16[256,1024]{1,0:T(8,128)(2,1)S(1)} %copy-done.7, ...), custom_call_target="tpu_custom_call" | custom-call | flops 4294967296 | bytes 1048576 | tf_op jit(solution)/shard_map/pallas_call | solution.py:504
  132.0 2.4 %collective-permute-start.39 = (bf16[48,384]{1,0:T(8,128)(2,1)S(1)}, bf16[48,384]{1,0:T(8,128)(2,1)S(1)}, u32[]{:S(2)}, u32[]{:S(2)}) collective-permute-start(bf16[48,384]{1,0:T(8,128)(2,1)S(1)} %shard_map.208), channel_id=1, source_target_pairs={{0,16},{4,20},{8,24},{12,28},{16,0},{20,4},{24,8},{28,12},{1,17},{... | collective-permute-start | bytes 110600 | tf_op jit(solution)/shard_map/ppermute | solution.py:23
  135.0 3.4 %shard_map.207 = (bf16[192,192]{1,0:T(8,128)(2,1)}, f32[192,192]{1,0:T(8,128)}, f32[192,384]{1,0:T(8,128)}) custom-call(bf16[192,384]{1,0:T(8,128)(2,1)} %copy-done.17, bf16[192,384]{1,0:T(8,128)(2,1)} %v_ref.3, bf16[192,192]{1,0:T(8,128)(2,1)} %q_ref.1, bf16[192,192]{1,0:T(8,128)(2,1)} %k_ref.3, f32[192,4]{1,0:T(8,128)} %get-tuple-element.67.sum_ref, ...), custom_call_target="tpu_custom_call" | custom-call | flops 4294967296 | bytes 1048576 | tf_op jit(solution)/shard_map/pallas_call | solution.py:326
  138.4 1.7 %collective-permute-done.40.refs_3_ = bf16[48,384]{1,0:T(8,128)(2,1)S(1)} collective-permute-done((bf16[48,384]{1,0:T(8,128)(2,1)S(1)}, bf16[48,384]{1,0:T(8,128)(2,1)S(1)}, u32[]{:S(2)}, u32[]{:S(2)}) %collective-permute-start.40) | collective-permute-done | bytes 36896 | tf_op jit(solution)/shard_map/ppermute | solution.py:23
  (152 shorter events, 42.0 us)
Async XLA Ops:
  3.7 19.9 %collective-permute-start.9 = (bf16[64,1024]{1,0:T(8,128)(2,1)}, bf16[64,1024]{1,0:T(8,128)(2,1)S(1)}, u32[]{:S(2)}, u32[]{:S(2)}) collective-permute-start(bf16[64,1024]{1,0:T(8,128)(2,1)} %get-tuple-element.52), channel_id=1, source_target_pairs={{0,16},{4,20},{8,24},{12,28},{16,0},{20,4},{24,8},{28,12},{1,17},{... | collective-permute-start | bytes 393224 | tf_op jit(solution)/shard_map/ppermute | solution.py:23
  7.9 19.8 %collective-permute-start.11 = (bf16[64,1024]{1,0:T(8,128)(2,1)}, bf16[64,1024]{1,0:T(8,128)(2,1)S(1)}, u32[]{:S(2)}, u32[]{:S(2)}) collective-permute-start(bf16[64,1024]{1,0:T(8,128)(2,1)} %get-tuple-element.53), channel_id=1, source_target_pairs={{0,20},{4,16},{8,28},{12,24},{16,4},{20,0},{24,12},{28,8},{1,21},{... | collective-permute-start | bytes 393224 | tf_op jit(solution)/shard_map/ppermute | solution.py:23
  9.1 20.1 %collective-permute-start.13 = (bf16[64,1024]{1,0:T(8,128)(2,1)}, bf16[64,1024]{1,0:T(8,128)(2,1)S(1)}, u32[]{:S(2)}, u32[]{:S(2)}) collective-permute-start(bf16[64,1024]{1,0:T(8,128)(2,1)} %get-tuple-element.54), channel_id=1, source_target_pairs={{0,24},{4,28},{8,16},{12,20},{16,8},{20,12},{24,0},{28,4},{1,25},{... | collective-permute-start | bytes 393224 | tf_op jit(solution)/shard_map/ppermute | solution.py:23
  12.7 17.0 %collective-permute-start.15 = (bf16[64,1024]{1,0:T(8,128)(2,1)}, bf16[64,1024]{1,0:T(8,128)(2,1)S(1)}, u32[]{:S(2)}, u32[]{:S(2)}) collective-permute-start(bf16[64,1024]{1,0:T(8,128)(2,1)} %get-tuple-element.55), channel_id=1, source_target_pairs={{0,28},{4,24},{8,20},{12,16},{16,12},{20,8},{24,4},{28,0},{1,29},{... | collective-permute-start | bytes 393224 | tf_op jit(solution)/shard_map/ppermute | solution.py:23
  23.7 7.6 %collective-permute-start.10 = (bf16[64,1024]{1,0:T(8,128)(2,1)S(1)}, bf16[64,1024]{1,0:T(8,128)(2,1)S(1)}, u32[]{:S(2)}, u32[]{:S(2)}) collective-permute-start(bf16[64,1024]{1,0:T(8,128)(2,1)S(1)} %collective-permute-done.9.refs_0_), channel_id=1, source_target_pairs={{0,2},{1,3},{2,0},{3,1},{4,6},{5,7},{6,4},{7,5},{8,10},{9,11},{10,... | collective-permute-start | bytes 393224 | tf_op jit(solution)/shard_map/ppermute | solution.py:23
  27.7 6.4 %collective-permute-start.12 = (bf16[64,1024]{1,0:T(8,128)(2,1)S(1)}, bf16[64,1024]{1,0:T(8,128)(2,1)S(1)}, u32[]{:S(2)}, u32[]{:S(2)}) collective-permute-start(bf16[64,1024]{1,0:T(8,128)(2,1)S(1)} %collective-permute-done.11.refs_2_), channel_id=1, source_target_pairs={{0,2},{1,3},{2,0},{3,1},{4,6},{5,7},{6,4},{7,5},{8,10},{9,11},{10,... | collective-permute-start | bytes 393224 | tf_op jit(solution)/shard_map/ppermute | solution.py:23
  29.2 6.4 %collective-permute-start.14 = (bf16[64,1024]{1,0:T(8,128)(2,1)S(1)}, bf16[64,1024]{1,0:T(8,128)(2,1)S(1)}, u32[]{:S(2)}, u32[]{:S(2)}) collective-permute-start(bf16[64,1024]{1,0:T(8,128)(2,1)S(1)} %collective-permute-done.13.refs_4_), channel_id=1, source_target_pairs={{0,2},{1,3},{2,0},{3,1},{4,6},{5,7},{6,4},{7,5},{8,10},{9,11},{10,... | collective-permute-start | bytes 393224 | tf_op jit(solution)/shard_map/ppermute | solution.py:23
  29.7 7.3 %collective-permute-start.16 = (bf16[64,1024]{1,0:T(8,128)(2,1)S(1)}, bf16[64,1024]{1,0:T(8,128)(2,1)S(1)}, u32[]{:S(2)}, u32[]{:S(2)}) collective-permute-start(bf16[64,1024]{1,0:T(8,128)(2,1)S(1)} %collective-permute-done.15.refs_6_), channel_id=1, source_target_pairs={{0,2},{1,3},{2,0},{3,1},{4,6},{5,7},{6,4},{7,5},{8,10},{9,11},{10,... | collective-permute-start | bytes 393224 | tf_op jit(solution)/shard_map/ppermute | solution.py:23
  37.1 18.0 %collective-permute-start.18 = (bf16[256,1024]{1,0:T(8,128)(2,1)S(1)}, bf16[256,1024]{1,0:T(8,128)(2,1)S(1)}, u32[]{:S(2)}, u32[]{:S(2)}) collective-permute-start(bf16[256,1024]{1,0:T(8,128)(2,1)S(1)} %get-tuple-element.57.refs_5_), channel_id=1, source_target_pairs={{0,1},{1,0},{2,3},{3,2},{4,5},{5,4},{6,7},{7,6},{8,9},{9,8},{10,11... | collective-permute-start | bytes 1572872 | tf_op jit(solution)/shard_map/ppermute | solution.py:23
  39.0 6.6 %collective-permute-start.3 = (bf16[64,1024]{1,0:T(8,128)(2,1)}, bf16[64,1024]{1,0:T(8,128)(2,1)S(1)}, u32[]{:S(2)}, u32[]{:S(2)}) collective-permute-start(bf16[64,1024]{1,0:T(8,128)(2,1)} %get-tuple-element.44), channel_id=1, source_target_pairs={{0,8},{4,12},{8,0},{12,4},{16,24},{20,28},{24,16},{28,20},{1,9},{5... | collective-permute-start | bytes 393224 | tf_op jit(solution)/shard_map/ppermute | solution.py:23
  39.6 7.7 %collective-permute-start.5 = (bf16[64,1024]{1,0:T(8,128)(2,1)}, bf16[64,1024]{1,0:T(8,128)(2,1)S(1)}, u32[]{:S(2)}, u32[]{:S(2)}) collective-permute-start(bf16[64,1024]{1,0:T(8,128)(2,1)} %get-tuple-element.45), channel_id=1, source_target_pairs={{0,12},{4,8},{8,4},{12,0},{16,28},{20,24},{24,20},{28,16},{1,13},{... | collective-permute-start | bytes 393224 | tf_op jit(solution)/shard_map/ppermute | solution.py:23
  40.8 11.3 %collective-permute-start = (bf16[64,1024]{1,0:T(8,128)(2,1)}, bf16[64,1024]{1,0:T(8,128)(2,1)S(1)}, u32[]{:S(2)}, u32[]{:S(2)}) collective-permute-start(bf16[64,1024]{1,0:T(8,128)(2,1)} %get-tuple-element.42.refs_0_), channel_id=1, source_target_pairs={{0,2},{1,3},{2,0},{3,1},{4,6},{5,7},{6,4},{7,5},{8,10},{9,11},{10,... | collective-permute-start | bytes 393224 | tf_op jit(solution)/shard_map/ppermute | solution.py:23
  43.3 8.8 %collective-permute-start.2 = (bf16[64,1024]{1,0:T(8,128)(2,1)S(1)}, bf16[64,1024]{1,0:T(8,128)(2,1)S(1)}, u32[]{:S(2)}, u32[]{:S(2)}) collective-permute-start(bf16[64,1024]{1,0:T(8,128)(2,1)S(1)} %collective-permute-done.1.refs_2_), channel_id=1, source_target_pairs={{0,2},{1,3},{2,0},{3,1},{4,6},{5,7},{6,4},{7,5},{8,10},{9,11},{10,... | collective-permute-start | bytes 393224 | tf_op jit(solution)/shard_map/ppermute | solution.py:23
  45.6 6.9 %collective-permute-start.4 = (bf16[64,1024]{1,0:T(8,128)(2,1)S(1)}, bf16[64,1024]{1,0:T(8,128)(2,1)S(1)}, u32[]{:S(2)}, u32[]{:S(2)}) collective-permute-start(bf16[64,1024]{1,0:T(8,128)(2,1)S(1)} %collective-permute-done.3.refs_4_), channel_id=1, source_target_pairs={{0,2},{1,3},{2,0},{3,1},{4,6},{5,7},{6,4},{7,5},{8,10},{9,11},{10,... | collective-permute-start | bytes 393224 | tf_op jit(solution)/shard_map/ppermute | solution.py:23
  47.3 7.2 %collective-permute-start.6 = (bf16[64,1024]{1,0:T(8,128)(2,1)S(1)}, bf16[64,1024]{1,0:T(8,128)(2,1)S(1)}, u32[]{:S(2)}, u32[]{:S(2)}) collective-permute-start(bf16[64,1024]{1,0:T(8,128)(2,1)S(1)} %collective-permute-done.5.refs_6_), channel_id=1, source_target_pairs={{0,2},{1,3},{2,0},{3,1},{4,6},{5,7},{6,4},{7,5},{8,10},{9,11},{10,... | collective-permute-start | bytes 393224 | tf_op jit(solution)/shard_map/ppermute | solution.py:23
  65.5 9.2 %collective-permute-start.25 = (bf16[256,512]{1,0:T(8,128)(2,1)S(1)}, bf16[256,512]{1,0:T(8,128)(2,1)S(1)}, u32[]{:S(2)}, u32[]{:S(2)}) collective-permute-start(bf16[256,512]{1,0:T(8,128)(2,1)S(1)} %add_convert_fusion.1), channel_id=1, source_target_pairs={{0,2},{1,3},{2,0},{3,1},{4,6},{5,7},{6,4},{7,5},{8,10},{9,11},{10,... | collective-permute-start | bytes 786440 | tf_op jit(solution)/shard_map/ppermute | solution.py:23
  67.8 15.0 %collective-permute-start.20 = (bf16[256,512]{1,0:T(8,128)(2,1)S(1)}, bf16[256,512]{1,0:T(8,128)(2,1)S(1)}, u32[]{:S(2)}, u32[]{:S(2)}) collective-permute-start(bf16[256,512]{1,0:T(8,128)(2,1)S(1)} %add_convert_fusion.3), channel_id=1, source_target_pairs={{0,2},{1,3},{2,0},{3,1},{4,6},{5,7},{6,4},{7,5},{8,10},{9,11},{10,... | collective-permute-start | bytes 786440 | tf_op jit(solution)/shard_map/ppermute | solution.py:23
  74.9 9.6 %collective-permute-start.26 = (bf16[64,512]{1,0:T(8,128)(2,1)S(1)}, bf16[64,512]{1,0:T(8,128)(2,1)S(1)}, u32[]{:S(2)}, u32[]{:S(2)}) collective-permute-start(bf16[64,512]{1,0:T(8,128)(2,1)S(1)} %get-tuple-element.86), channel_id=1, source_target_pairs={{0,16},{4,20},{8,24},{12,28},{16,0},{20,4},{24,8},{28,12},{1,17},{... | collective-permute-start | bytes 196616 | tf_op jit(solution)/shard_map/ppermute | solution.py:23
  78.0 9.4 %collective-permute-start.27 = (bf16[64,512]{1,0:T(8,128)(2,1)S(1)}, bf16[64,512]{1,0:T(8,128)(2,1)S(1)}, u32[]{:S(2)}, u32[]{:S(2)}) collective-permute-start(bf16[64,512]{1,0:T(8,128)(2,1)S(1)} %get-tuple-element.85), channel_id=1, source_target_pairs={{0,20},{4,16},{8,28},{12,24},{16,4},{20,0},{24,12},{28,8},{1,21},{... | collective-permute-start | bytes 196616 | tf_op jit(solution)/shard_map/ppermute | solution.py:23
  78.9 8.5 %collective-permute-start.28 = (bf16[64,512]{1,0:T(8,128)(2,1)S(1)}, bf16[64,512]{1,0:T(8,128)(2,1)S(1)}, u32[]{:S(2)}, u32[]{:S(2)}) collective-permute-start(bf16[64,512]{1,0:T(8,128)(2,1)S(1)} %get-tuple-element.84), channel_id=1, source_target_pairs={{0,24},{4,28},{8,16},{12,20},{16,8},{20,12},{24,0},{28,4},{1,25},{... | collective-permute-start | bytes 196616 | tf_op jit(solution)/shard_map/ppermute | solution.py:23
  81.8 7.7 %collective-permute-start.29 = (bf16[64,512]{1,0:T(8,128)(2,1)S(1)}, bf16[64,512]{1,0:T(8,128)(2,1)S(1)}, u32[]{:S(2)}, u32[]{:S(2)}) collective-permute-start(bf16[64,512]{1,0:T(8,128)(2,1)S(1)} %get-tuple-element.83), channel_id=1, source_target_pairs={{0,28},{4,24},{8,20},{12,16},{16,12},{20,8},{24,4},{28,0},{1,29},{... | collective-permute-start | bytes 196616 | tf_op jit(solution)/shard_map/ppermute | solution.py:23
  83.0 6.6 %collective-permute-start.21 = (bf16[64,512]{1,0:T(8,128)(2,1)S(1)}, bf16[64,512]{1,0:T(8,128)(2,1)S(1)}, u32[]{:S(2)}, u32[]{:S(2)}) collective-permute-start(bf16[64,512]{1,0:T(8,128)(2,1)S(1)} %get-tuple-element.89), channel_id=1, source_target_pairs={{0,4},{4,0},{8,12},{12,8},{16,20},{20,16},{24,28},{28,24},{1,5},{5... | collective-permute-start | bytes 196616 | tf_op jit(solution)/shard_map/ppermute | solution.py:23
  93.3 6.5 %collective-permute-start.30 = (bf16[192,512]{1,0:T(8,128)(2,1)S(1)}, bf16[192,512]{1,0:T(8,128)(2,1)S(1)}, u32[]{:S(2)}, u32[]{:S(2)}) collective-permute-start(bf16[192,512]{1,0:T(8,128)(2,1)S(1)} %shard_map.202), channel_id=1, source_target_pairs={{0,2},{1,3},{2,0},{3,1},{4,6},{5,7},{6,4},{7,5},{8,10},{9,11},{10,... | collective-permute-start | bytes 589832 | tf_op jit(solution)/shard_map/ppermute | solution.py:23
  94.8 7.8 %collective-permute-start.33 = (bf16[1,208,384]{2,1,0:T(8,128)(2,1)S(1)}, bf16[1,208,384]{2,1,0:T(8,128)(2,1)S(1)}, u32[]{:S(2)}, u32[]{:S(2)}) collective-permute-start(bf16[1,208,384]{2,1,0:T(8,128)(2,1)S(1)} %copy-done.30), channel_id=1, source_target_pairs={{0,8},{4,12},{8,0},{12,4},{16,24},{20,28},{24,16},{28,20},{1,9},{5... | collective-permute-start | bytes 479240 | tf_op jit(solution)/shard_map/ppermute | solution.py:23
  94.8 12.3 %collective-permute-start.34 = (bf16[1,208,384]{2,1,0:T(8,128)(2,1)S(1)}, bf16[1,208,384]{2,1,0:T(8,128)(2,1)S(1)}, u32[]{:S(2)}, u32[]{:S(2)}) collective-permute-start(bf16[1,208,384]{2,1,0:T(8,128)(2,1)S(1)} %copy-done.30), channel_id=1, source_target_pairs={{0,16},{4,20},{8,24},{12,28},{16,0},{20,4},{24,8},{28,12},{1,17},{... | collective-permute-start | bytes 479240 | tf_op jit(solution)/shard_map/ppermute | solution.py:23
  99.8 7.4 %collective-permute-start.35 = (bf16[1,208,384]{2,1,0:T(8,128)(2,1)S(1)}, bf16[1,208,384]{2,1,0:T(8,128)(2,1)S(1)}, u32[]{:S(2)}, u32[]{:S(2)}) collective-permute-start(bf16[1,208,384]{2,1,0:T(8,128)(2,1)S(1)} %copy-done.30), channel_id=1, source_target_pairs={{0,24},{4,28},{8,16},{12,20},{16,8},{20,12},{24,0},{28,4},{1,25},{... | collective-permute-start | bytes 479240 | tf_op jit(solution)/shard_map/ppermute | solution.py:23
  99.9 9.4 %collective-permute-start.31 = (bf16[192,1024]{1,0:T(8,128)(2,1)S(1)}, bf16[192,1024]{1,0:T(8,128)(2,1)S(1)}, u32[]{:S(2)}, u32[]{:S(2)}) collective-permute-start(bf16[192,1024]{1,0:T(8,128)(2,1)S(1)} %pad_maximum_fusion.2.mine_ref), channel_id=1, source_target_pairs={{0,1},{1,0},{2,3},{3,2},{4,5},{5,4},{6,7},{7,6},{8,9},{9,8},{10,11... | collective-permute-start | bytes 1179656 | tf_op jit(solution)/shard_map/ppermute | solution.py:23
  107.2 23.1 %collective-permute-start.36 = (bf16[4,208,384]{2,1,0:T(8,128)(2,1)S(1)}, bf16[4,208,384]{2,1,0:T(8,128)(2,1)S(1)}, u32[]{:S(2)}, u32[]{:S(2)}) collective-permute-start(bf16[4,208,384]{2,1,0:T(8,128)(2,1)S(1)} %constant_dynamic-update-slice_fusion.wide_ref), channel_id=1, source_target_pairs={{0,4},{4,0},{8,12},{12,8},{16,20},{20,16},{24,28},{28,24},{1,5},{5... | collective-permute-start | bytes 1916936 | tf_op jit(solution)/shard_map/ppermute | solution.py:23
  111.8 23.1 %all-to-all-start = ((bf16[8,96,256]{2,1,0:T(8,128)(2,1)}), bf16[8,96,256]{2,1,0:T(8,128)(2,1)S(1)}, u32[]{:S(2)}, u32[]{:S(2)}) async-start(bf16[8,96,256]{2,1,0:T(8,128)(2,1)} %copy-done.8), calls=%async_computation | async-start | bytes 786432 | tf_op jit(solution)/shard_map/all_to_all | solution.py:578
  130.5 7.9 %collective-permute-start.38 = (bf16[48,384]{1,0:T(8,128)(2,1)S(1)}, bf16[48,384]{1,0:T(8,128)(2,1)S(1)}, u32[]{:S(2)}, u32[]{:S(2)}) collective-permute-start(bf16[48,384]{1,0:T(8,128)(2,1)S(1)} %shard_map.208), channel_id=1, source_target_pairs={{0,8},{4,12},{8,0},{12,4},{16,24},{20,28},{24,16},{28,20},{1,9},{5... | collective-permute-start | bytes 110600 | tf_op jit(solution)/shard_map/ppermute | solution.py:23
  132.0 6.4 %collective-permute-start.39 = (bf16[48,384]{1,0:T(8,128)(2,1)S(1)}, bf16[48,384]{1,0:T(8,128)(2,1)S(1)}, u32[]{:S(2)}, u32[]{:S(2)}) collective-permute-start(bf16[48,384]{1,0:T(8,128)(2,1)S(1)} %shard_map.208), channel_id=1, source_target_pairs={{0,16},{4,20},{8,24},{12,28},{16,0},{20,4},{24,8},{28,12},{1,17},{... | collective-permute-start | bytes 110600 | tf_op jit(solution)/shard_map/ppermute | solution.py:23
  135.0 8.5 %collective-permute-start.32 = (bf16[8,96,256]{2,1,0:T(8,128)(2,1)S(1)}, bf16[8,96,256]{2,1,0:T(8,128)(2,1)S(1)}, u32[]{:S(2)}, u32[]{:S(2)}) collective-permute-start(bf16[8,96,256]{2,1,0:T(8,128)(2,1)S(1)} %all-to-all-done), channel_id=1, source_target_pairs={{0,1},{1,0},{2,3},{3,2},{4,5},{5,4},{6,7},{7,6},{8,9},{9,8},{10,11... | collective-permute-start | bytes 1179656 | tf_op jit(solution)/shard_map/ppermute | solution.py:23
  (41 other events, 300.0 us)
